TPU v7x, 256 devices: a whole 4x4x8 slice. The times are simulated.
256 devices in a mesh: sp: 16 (over y, x), tp: 16 (over z, core).
Axes of the slice: x: 4, y: 4, z: 8, core: 2. Of those that a mesh axis runs over, the one named last changes fastest.
Arguments:
- query_first: bfloat16 [8192, 1536], P('sp', 'tp'), may hold values from -10 to 10
- query_second: bfloat16 [8192, 2560], P('sp', 'tp'), may hold values from -10 to 10
- latent: bfloat16 [8192, 512], P('sp'), may hold values from -400 to 400
- key_rotary: bfloat16 [8192, 32], P('sp'), may hold values from -90 to 90
- latent_gain: float32 [512], replicated, may hold values from 0.1 to 1.9
- key_up_first: bfloat16 [512, 1024], P(None, 'tp'), may hold values from -0.25 to 0.25
- value_up_first: bfloat16 [512, 1024], P(None, 'tp'), may hold values from -0.25 to 0.25
- key_up_second: bfloat16 [512, 2048], P(None, 'tp'), may hold values from -0.25 to 0.25
- value_up_second: bfloat16 [512, 2048], P(None, 'tp'), may hold values from -0.25 to 0.25
- out_first: bfloat16 [1024, 2048], P('tp'), may hold values from -0.109375 to 0.109375
- out_second: bfloat16 [2048, 2048], P('tp'), may hold values from -0.109375 to 0.109375
- residual: bfloat16 [8192, 2048], P('sp'), may hold values from -16 to 16
- expert_gain: float32 [2048], replicated, may hold values from 0.1 to 1.9
- route_experts: int32 [8192, 2], P('sp'), may hold values from 0 to 31, all different within a row; in each aligned block of 32 rows (0 to 31, 32 to 63, ...) at most 3 rows name the same one
- route_scores: float32 [8192, 2], P('sp'), may hold values from -6 to 306
- gate_weight: bfloat16 [32, 2048, 4096], P('sp', None, 'tp'), may hold values from -0.375 to 0.375
- up_weight: bfloat16 [32, 2048, 4096], P('sp', None, 'tp'), may hold values from -0.375 to 0.375
- down_weight: bfloat16 [32, 4096, 2048], P('sp', 'tp'), may hold values from -0.013671875 to 0.013671875
Outputs:
- mixed: bfloat16 [8192, 2048], P(('sp', 'tp'))
Inputs may be any that keep to these rules, and one draw needn't show every extreme that they name: `route_experts`: each row names 2 different experts. In every aligned block of 32 rows no expert is named more than 3 times, and in some blocks one is named exactly 3 times.
All inputs are finite; a program needn't handle non-finite values.
Results may differ from a plain program's by a relative error of at most 0.02.
The roundings to bfloat16 on the way count: a program that leaves them out, or rounds other values in their place, can miss the bound.
Values may be sent and summed in bfloat16 or wider, within the bound.
A program may use at most 128 MiB of HBM per device.

v0:
```python
import jax
import jax.numpy as jnp
from jax import lax
from jax.sharding import PartitionSpec as P

NA = 64
NB = 128
ROPE = 32
CAP = 3


norm_epsilon = 1e-06
rotary_base = 10000.0
clamp_limit = 7.0
sigmoid_slope = 1.702
masked_score = -1e30


def in_one_piece(arrays, axis, dim, along):
    ends, at = ([], 0)
    for a in arrays[:-1]:
        at += a.shape[along]
        ends.append(at)
    both = jnp.concatenate(arrays, axis=along)
    return tuple(jnp.split(lax.all_gather(both, axis, axis=dim, tiled=True), ends, axis=along))


def in_blocks(value, dim, count):
    before, after = (value.shape[:dim], value.shape[dim + 1 :])
    return jnp.moveaxis(value.reshape(*before, count, -1, *after), dim, 0)


def sum_at_owner(value, axis, dim):
    tiles = in_blocks(value, dim, lax.axis_size(axis))
    arrived = lax.all_to_all(tiles, axis, split_axis=0, concat_axis=0, tiled=True)
    return arrived.astype(jnp.float32).sum(axis=0)


def rotate(values, positions):
    half = values.shape[-1] // 2
    inverse = rotary_base ** (-jnp.arange(half, dtype=jnp.float32) / half)
    angles = positions.astype(jnp.float32)[:, None, None] * inverse[None, None, :]
    cosine = jnp.cos(angles)
    sine = jnp.sin(angles)
    first = values[..., :half]
    second = values[..., half:]
    return jnp.concatenate(
        [first * cosine - second * sine, second * cosine + first * sine], axis=-1
    )


def rms_scaled(values, gain):
    wide = values.astype(jnp.float32)
    return wide * lax.rsqrt(jnp.mean(wide * wide, axis=-1, keepdims=True) + norm_epsilon) * gain


def turned_queries(query, nope, positions):
    shaped = query.reshape(query.shape[0], query.shape[1] // (nope + ROPE), nope + ROPE)
    turned = rotate(shaped[..., nope:].astype(jnp.float32), positions).astype(jnp.bfloat16)
    return jnp.concatenate([shaped[..., :nope], turned], axis=-1)


def clamped_unit(gate, upward):
    limited = jnp.minimum(gate, clamp_limit)
    bounded = jnp.clip(upward, -clamp_limit, clamp_limit)
    return (bounded + 1.0) * limited * jax.nn.sigmoid(sigmoid_slope * limited)


def slot_numbers(chosen, experts):
    hits = (chosen[..., None] == jnp.arange(experts, dtype=jnp.int32)).astype(jnp.int32)
    before = jnp.cumsum(hits, axis=-2) - hits
    return chosen * CAP + jnp.sum(before * hits, axis=-1)


def fold_group(state, queries, key_nope, key_turned, values, query_places, scale):
    running, denominator, numerator = state
    heads = queries.shape[1]
    nope = queries.shape[2] - key_turned.shape[1]
    keys = key_nope.reshape(key_nope.shape[0], heads, nope)
    value_rows = values.reshape(values.shape[0], heads, values.shape[1] // heads)
    score = jnp.einsum(
        "qhd,khd->qhk", queries[..., :nope], keys, preferred_element_type=jnp.float32
    )
    score = score + jnp.einsum(
        "qhr,kr->qhk", queries[..., nope:], key_turned, preferred_element_type=jnp.float32
    )
    score = score * scale
    key_places = jnp.arange(keys.shape[0], dtype=jnp.int32)
    allowed = (query_places[:, None] >= key_places[None, :])[:, None, :]
    score = jnp.where(allowed, score, masked_score)
    highest = jnp.maximum(running, jnp.max(score, axis=-1))
    weights = jnp.where(allowed, jnp.exp(score - highest[..., None]), 0.0)
    denominator = jnp.sum(weights, axis=-1)
    numerator = jnp.einsum(
        "qhk,khd->qhd", weights.astype(jnp.bfloat16), value_rows, preferred_element_type=jnp.float32
    )
    return (highest, denominator, numerator)


def expert_hidden(rows, gate_weight, up_weight):
    gate = jnp.einsum("nsecd,edf->nsecf", rows, gate_weight, preferred_element_type=jnp.float32)
    upward = jnp.einsum("nsecd,edf->nsecf", rows, up_weight, preferred_element_type=jnp.float32)
    return clamped_unit(gate, upward).astype(jnp.bfloat16)


def body(
    query_first,
    query_second,
    latent,
    key_rotary,
    latent_gain,
    key_up_first,
    value_up_first,
    key_up_second,
    value_up_second,
    out_first,
    out_second,
    residual,
    expert_gain,
    route_experts,
    route_scores,
    gate_weight,
    up_weight,
    down_weight,
):
    seq_rows = latent.shape[0]
    sets = lax.axis_size("tp")
    groups = lax.axis_size("sp")
    own_rows = seq_rows // sets
    topk = route_experts.shape[1]
    local_experts = gate_weight.shape[0]
    experts = local_experts * groups
    offset = lax.axis_index("sp") * seq_rows
    places = offset + jnp.arange(seq_rows, dtype=jnp.int32)
    last_place = offset + seq_rows - 1
    queries_first = turned_queries(query_first, NA, places)
    queries_second = turned_queries(query_second, NB, places)
    key_turned = rotate(key_rotary.astype(jnp.float32)[:, None, :], places)[:, 0, :].astype(
        jnp.bfloat16
    )
    latent_normed = rms_scaled(latent, latent_gain).astype(jnp.bfloat16)
    scale_first = (NA + ROPE) ** (-0.5)
    scale_second = (NB + ROPE) ** (-0.5)

    def attend(carry, parts):
        key_first, value_first, key_second, value_second, turned = parts
        return (
            fold_group(
                carry[0], queries_first, key_first, turned, value_first, places, scale_first
            ),
            fold_group(
                carry[1], queries_second, key_second, turned, value_second, places, scale_second
            ),
        )

    def initial(queries, value_width):
        shape = queries.shape[:2]
        return (
            jnp.full(shape, masked_score, jnp.float32),
            jnp.zeros(shape, jnp.float32),
            jnp.zeros(shape + (value_width,), jnp.float32),
        )

    start_state = (
        initial(queries_first, value_up_first.shape[1] // queries_first.shape[1]),
        initial(queries_second, value_up_second.shape[1] // queries_second.shape[1]),
    )
    key_first, value_first, key_second, value_second = tuple(
        (
            jnp.dot(latent_normed, weight, preferred_element_type=jnp.float32).astype(jnp.bfloat16)
            for weight in (key_up_first, value_up_first, key_up_second, value_up_second)
        )
    )
    parts = in_one_piece((key_first, value_first, key_second, value_second, key_turned), "sp", 0, 1)
    state = lax.cond(
        jnp.int32(0) <= last_place,
        lambda inner: attend(inner, parts),
        lambda inner: inner,
        start_state,
    )
    first_state, second_state = state
    attended_first = (
        (first_state[2] / first_state[1][..., None]).astype(jnp.bfloat16).reshape(seq_rows, -1)
    )
    attended_second = (
        (second_state[2] / second_state[1][..., None]).astype(jnp.bfloat16).reshape(seq_rows, -1)
    )
    own_start = lax.axis_index("tp") * own_rows
    slot_range = jnp.arange(experts * CAP, dtype=jnp.int32)
    projected = sum_at_owner(
        (
            jnp.dot(attended_first, out_first, preferred_element_type=jnp.float32)
            + jnp.dot(attended_second, out_second, preferred_element_type=jnp.float32)
        ).astype(jnp.bfloat16),
        "tp",
        0,
    )
    own_residual = lax.dynamic_slice_in_dim(residual, own_start, own_rows, 0)
    middle = (own_residual.astype(jnp.float32) + projected).astype(jnp.bfloat16)
    normed = rms_scaled(middle, expert_gain).astype(jnp.bfloat16)
    own_ids = lax.dynamic_slice_in_dim(route_experts, own_start, own_rows, 0).reshape(-1)
    own_slots = slot_numbers(own_ids, experts)
    picks = (own_slots[:, None] == slot_range).reshape(own_rows, topk, experts * CAP)
    selected = jnp.sum(picks.astype(jnp.float32), axis=1).astype(jnp.bfloat16)
    outgoing = jnp.einsum("ts,td->sd", selected, normed, preferred_element_type=jnp.float32).astype(
        jnp.bfloat16
    )
    outgoing = outgoing.reshape(groups, local_experts, CAP, outgoing.shape[-1])
    arrived = lax.all_to_all(outgoing, "sp", split_axis=0, concat_axis=0, tiled=True)
    activated = expert_hidden(
        lax.all_gather(arrived[None], "tp", axis=0, tiled=True), gate_weight, up_weight
    )
    flat_hidden = activated.reshape(sets * groups, local_experts, CAP, activated.shape[-1])
    summed = lax.psum_scatter(
        jnp.einsum(
            "secf,efd->secd", flat_hidden, down_weight, preferred_element_type=jnp.float32
        ).astype(jnp.bfloat16),
        "tp",
        scatter_dimension=0,
        tiled=True,
    )
    returned = lax.all_to_all(summed, "sp", split_axis=0, concat_axis=0, tiled=True)
    expert_out = returned.reshape(experts * CAP, returned.shape[-1]).astype(jnp.float32)
    own_scores = lax.dynamic_slice_in_dim(route_scores, own_start, own_rows, 0)
    route_weight = jax.nn.softmax(own_scores, axis=-1)
    matches = own_slots.reshape(own_rows, topk)[..., None] == slot_range
    combine = jnp.sum(jnp.where(matches, route_weight[..., None], 0.0), axis=1)
    mixture = jnp.dot(combine, expert_out)
    return (middle.astype(jnp.float32) + mixture).astype(jnp.bfloat16)


def solution(mesh):
    in_specs = (
        P("sp", "tp"),
        P("sp", "tp"),
        P("sp", None),
        P("sp", None),
        P(),
        P(None, "tp"),
        P(None, "tp"),
        P(None, "tp"),
        P(None, "tp"),
        P("tp", None),
        P("tp", None),
        P("sp", None),
        P(),
        P("sp", None),
        P("sp", None),
        P("sp", None, "tp"),
        P("sp", None, "tp"),
        P("sp", "tp", None),
    )
    out_specs = P(("sp", "tp"), None)
    return jax.shard_map(body, mesh=mesh, in_specs=in_specs, out_specs=out_specs, check_vma=False)
```

profile of v0, /device:TPU:2, one launch (start us, length us, event | category | flops | bytes accessed | tf_op | source)
XLA Modules:
  0.0 388.1 jit_solution(6274930086151331224)
XLA Ops:
  13.1 1.5 fusion.56
  17.2 77.3 %all-gather.4.cloned.1.call-done = bf16[8192,416]{0,1:T(8,128)(2,1)} async-done(((bf16[512,416]{0,1:T(8,128)(2,1)}), bf16[8192,416]{0,1:T(8,128)(2,1)}) %all-gather.4.cloned.1.call-update) | async-done | bytes 6815760 | tf_op jit(solution)/shard_map/all_gather | solution.py:25
  94.5 66.5 %conditional.1 = (f32[512,1]{0,1:T(1,128)S(1)}, f32[512,1,64]{0,2,1:T(8,128)S(1)}, f32[512,1]{0,1:T(1,128)S(1)}, f32[512,1,128]{2,0,1:T(8,128)S(1)}) conditional(s32[]{:T(128)} %convert_element_type.116, () %tuple.13, (s32[]{:T(128)}, s32[512]{0:T(512)S(1)}, bf16[8192,416]{0,1:T(8,128)(2,1)}, bf16[512,1,96]{0,2,1:T(8,128)(2,1)}, ...), branch_computations={%region_1.0_spmd, %region_2.7_spmd} | conditional | flops 3862953472 | bytes 245733568 | solution.py:175
  95.5 10.8 %copy.66 = bf16[8192,416]{1,0:T(8,128)(2,1)} copy(bf16[8192,416]{0,1:T(8,128)(2,1)} %get-tuple-element.77) | data formatting | bytes 13631488 | tf_op jit(solution)/shard_map
  106.3 3.9 %fusion.15 = f32[8192,512]{1,0:T(8,128)S(1)} fusion(bf16[8192,416]{1,0:T(8,128)(2,1)} %copy.66, bf16[512,1,160]{2,0,1:T(8,128)(2,1)S(1)} %copy.67), kind=kOutput, calls=%fused_computation.18 | convolution fusion | flops 1073741824 | bytes 19005440 | tf_op jit(solution)/shard_map/cond/branch_1_fun/qhd,khd->qhk/dot_general | solution.py:81
  110.3 9.4 %fusion.105 = (f32[512]{0:T(512)S(1)}, f32[512,1,8192]{0,2,1:T(8,128)}) fusion(bf16[512,1,32]{0,2,1:T(8,128)(2,1)S(1)} %get-tuple-element.38, bf16[8192,416]{1,0:T(8,128)(2,1)} %copy.66, f32[8192,512]{1,0:T(8,128)S(1)} %fusion.15, s32[512]{0:T(512)S(1)} %broadcast_add_fusion), kind=kOutput, calls=%fused_computation.129 | convolution fusion | flops 289406464 | bytes 35688448 | tf_op jit(solution)/shard_map/cond/branch_1_fun/qhr,kr->qhk/dot_general | solution.py:84
  119.7 3.9 %fusion.18 = f32[8192,512]{1,0:T(8,128)S(1)} fusion(bf16[8192,416]{1,0:T(8,128)(2,1)} %copy.66, bf16[512,1,96]{0,2,1:T(8,128)(2,1)S(1)} %copy-done.2), kind=kOutput, calls=%fused_computation.21 | convolution fusion | flops 536870912 | bytes 18939904 | tf_op jit(solution)/shard_map/cond/branch_1_fun/qhd,khd->qhk/dot_general | solution.py:81
  123.6 9.4 %fusion.106 = (f32[512]{0:T(512)S(1)}, f32[512,1,8192]{0,2,1:T(8,128)}) fusion(bf16[512,1,32]{0,2,1:T(8,128)(2,1)S(1)} %get-tuple-element.36, bf16[8192,416]{1,0:T(8,128)(2,1)} %copy.66, f32[8192,512]{1,0:T(8,128)S(1)} %fusion.18, s32[512]{0:T(512)S(1)} %broadcast_add_fusion), kind=kOutput, calls=%fused_computation.130 | convolution fusion | flops 289406464 | bytes 35688448 | tf_op jit(solution)/shard_map/cond/branch_1_fun/qhr,kr->qhk/dot_general | solution.py:84
  133.0 13.8 %fusion.7 = (f32[512]{0:T(512)S(1)}, f32[512]{0:T(512)S(1)}) fusion(f32[512,1,8192]{0,2,1:T(8,128)} %get-tuple-element.89, f32[512]{0:T(512)S(1)} %get-tuple-element.92, s32[512]{0:T(512)S(1)} %broadcast_add_fusion, f32[512,1,8192]{0,2,1:T(8,128)} %get-tuple-element.91, f32[512]{0:T(512)S(1)} %get-tuple-element.93), kind=kLoop, calls=%fused_computation.12 | loop fusion | flops 29359104 | bytes 33564672 | tf_op jit(solution)/shard_map/cond/branch_1_fun/reduce_sum | solution.py:93
  146.9 9.0 %fusion.27 = f32[512,1,64]{0,2,1:T(8,128)S(1)} fusion(bf16[8192,416]{1,0:T(8,128)(2,1)} %copy.66, f32[512,1,8192]{0,2,1:T(8,128)} %get-tuple-element.91, f32[512]{0:T(512)S(1)} %get-tuple-element.93, s32[512]{0:T(512)S(1)} %broadcast_add_fusion), kind=kOutput, calls=%fused_computation.26 | convolution fusion | flops 553648128 | bytes 19009536 | tf_op jit(solution)/shard_map/cond/branch_1_fun/qhk,khd->qhd/dot_general | solution.py:94
  155.9 5.1 %fusion.22 = f32[512,1,128]{2,0,1:T(8,128)S(1)} fusion(bf16[8192,416]{1,0:T(8,128)(2,1)} %copy.66, f32[512,1,8192]{0,2,1:T(8,128)S(1)} %bitcast.114, f32[512]{0:T(512)S(1)} %get-tuple-element.92, s32[512]{0:T(512)S(1)} %broadcast_add_fusion), kind=kOutput, calls=%fused_computation.25 | convolution fusion | flops 1090519040 | bytes 19140608 | tf_op jit(solution)/shard_map/cond/branch_1_fun/qhk,khd->qhd/dot_general | solution.py:94
  161.0 1.8 fusion.66
  162.8 3.0 add_convert_fusion
  165.8 7.2 %all-to-all-start = ((bf16[16,32,2048]{2,1,0:T(8,128)(2,1)}), bf16[16,32,2048]{2,1,0:T(8,128)(2,1)}, u32[]{:S(2)}, u32[]{:S(2)}) async-start(bf16[16,32,2048]{2,1,0:T(8,128)(2,1)} %bitcast.115), calls=%async_computation | async-start | bytes 4194304 | tf_op jit(solution)/shard_map/all_to_all | solution.py:35
  174.9 47.3 %all-to-all-done = bf16[16,32,2048]{2,1,0:T(8,128)(2,1)} async-done(((bf16[16,32,2048]{2,1,0:T(8,128)(2,1)}), bf16[16,32,2048]{2,1,0:T(8,128)(2,1)}, u32[]{:S(2)}, u32[]{:S(2)}) %all-to-all-start) | async-done | bytes 2097184 | tf_op jit(solution)/shard_map/all_to_all | solution.py:35
  222.3 2.0 convert_reduce_fusion
  226.4 14.7 %all_to_all.15 = bf16[16,2,3,2048]{3,1,2,0:T(2,128)(2,1)} all-to-all(bf16[16,2,3,2048]{3,1,2,0:T(2,128)(2,1)S(1)} %copy.70), channel_id=1, replica_groups=mesh['sp'=16,'tp'=16] {'sp'}, dimensions={0} | all-to-all | bytes 786432 | tf_op jit(solution)/shard_map/all_to_all | solution.py:209
  241.4 41.8 %all-gather.6.cloned.1.call-done = bf16[256,2,3,2048]{3,1,2,0:T(2,128)(2,1)} async-done(((bf16[16,2,3,2048]{3,1,2,0:T(2,128)(2,1)}), bf16[256,2,3,2048]{3,1,2,0:T(2,128)(2,1)}) %all-gather.6.cloned.1.call-update) | async-done | bytes 6291472 | tf_op jit(solution)/shard_map/all_gather | solution.py:211
  283.3 5.8 %copy.71 = bf16[256,2,3,2048]{3,0,2,1:T(8,128)(2,1)S(1)} copy(bf16[256,2,3,2048]{3,1,2,0:T(2,128)(2,1)} %all-gather.6.cloned.1.call-done) | data formatting | bytes 12582912 | tf_op jit(solution)/shard_map/all_gather | solution.py:211
  289.1 1.8 fusion.38
  290.9 2.2 fusion.50
  293.2 4.5 %convert_bitcast_fusion = bf16[256,2,3,2048]{3,0,2,1:T(8,128)(2,1)} fusion(bf16[256,2,3,256]{3,0,2,1:T(8,128)(2,1)S(1)} %bitcast.118, bf16[2,256,2048]{2,1,0:T(8,128)(2,1)S(1)} %copy-done), kind=kOutput, calls=%fused_computation.37 | convolution fusion | flops 1613758464 | bytes 9175040 | tf_op jit(solution)/shard_map/secf,efd->secd/dot_general | solution.py:215
  297.7 65.9 %reduce-scatter.2.cloned.1.call-done = bf16[16,2,3,2048]{3,0,2,1:T(8,128)(2,1)} async-done(((bf16[256,2,3,2048]{3,0,2,1:T(8,128)(2,1)}), bf16[16,2,3,2048]{3,0,2,1:T(8,128)(2,1)}) %reduce-scatter.2.cloned.1.call-update) | async-done | bytes 393232 | tf_op jit(solution)/shard_map/reduce_scatter | solution.py:214
  365.0 15.1 %all_to_all.16 = bf16[16,2,3,2048]{3,1,2,0:T(2,128)(2,1)S(1)} all-to-all(bf16[16,2,3,2048]{3,1,2,0:T(2,128)(2,1)S(1)} %copy.75), channel_id=1, replica_groups=mesh['sp'=16,'tp'=16] {'sp'}, dimensions={0} | all-to-all | bytes 786432 | tf_op jit(solution)/shard_map/all_to_all | solution.py:222
  (69 shorter events, 17.4 us)
Async XLA Ops:
  6.5 286.6 %copy-start = (bf16[2,256,2048]{2,1,0:T(8,128)(2,1)S(1)}, bf16[2,256,2048]{2,1,0:T(8,128)(2,1)}, u32[]{:S(2)}) copy-start(bf16[2,256,2048]{2,1,0:T(8,128)(2,1)} %param.37) | copy-start | bytes 6291460
  6.5 87.9 %all-gather.4.cloned.1.call-start = ((), (), s32[]{:S(2)}) async-start(), calls=%async_computation.4 | async-start | bytes 7241728 | tf_op jit(solution)/shard_map/all_gather | solution.py:25
  16.4 0.8 copy-start.1
  110.2 9.5 %copy-start.2 = (bf16[512,1,96]{0,2,1:T(8,128)(2,1)S(1)}, bf16[512,1,96]{0,2,1:T(8,128)(2,1)}, u32[]{:S(2)}) copy-start(bf16[512,1,96]{0,2,1:T(8,128)(2,1)} %get-tuple-element.35) | copy-start | bytes 294916 | tf_op jit(solution)/shard_map/cond
  133.0 22.8 %slice-start = ((s8[16777216]{0:T(1024)(128)(4,1)}), s8[4194304]{0:T(1024)(128)(4,1)S(1)}, s32[]{:S(2)}) async-start(s8[16777216]{0:T(1024)(128)(4,1)} %bitcast.113), calls=%async_computation.7 | async-start | bytes 8388608 | tf_op jit(solution)/shard_map/cond
  133.0 22.8 %slice-start.1 = ((s8[16777216]{0:T(1024)(128)(4,1)}), s8[4194304]{0:T(1024)(128)(4,1)S(1)}, s32[]{:S(2)}) async-start(s8[16777216]{0:T(1024)(128)(4,1)} %bitcast.113), calls=%async_computation.8 | async-start | bytes 8388608 | tf_op jit(solution)/shard_map/cond
  133.0 22.8 %slice-start.2 = ((s8[16777216]{0:T(1024)(128)(4,1)}), s8[4194304]{0:T(1024)(128)(4,1)S(1)}, s32[]{:S(2)}) async-start(s8[16777216]{0:T(1024)(128)(4,1)} %bitcast.113), calls=%async_computation.9 | async-start | bytes 8388608 | tf_op jit(solution)/shard_map/cond
  146.9 9.0 %slice-start.3 = ((s8[16777216]{0:T(1024)(128)(4,1)}), s8[4194304]{0:T(1024)(128)(4,1)S(1)}, s32[]{:S(2)}) async-start(s8[16777216]{0:T(1024)(128)(4,1)} %bitcast.113), calls=%async_computation.10 | async-start | bytes 8388608 | tf_op jit(solution)/shard_map/cond
  161.0 12.1 %copy-start.4 = (f32[512,2]{0,1:T(2,128)S(1)}, f32[512,2]{0,1:T(2,128)}, u32[]{:S(2)}) copy-start(f32[512,2]{0,1:T(2,128)} %param.34) | copy-start | bytes 12292
  161.0 64.4 %copy-start.3 = (f32[2048]{0:T(1024)S(1)}, f32[2048]{0:T(1024)}, u32[]{:S(2)}) copy-start(f32[2048]{0:T(1024)} %param.32) | copy-start | bytes 24580
  165.8 56.5 %all-to-all-start = ((bf16[16,32,2048]{2,1,0:T(8,128)(2,1)}), bf16[16,32,2048]{2,1,0:T(8,128)(2,1)}, u32[]{:S(2)}, u32[]{:S(2)}) async-start(bf16[16,32,2048]{2,1,0:T(8,128)(2,1)} %bitcast.115), calls=%async_computation | async-start | bytes 4194304 | tf_op jit(solution)/shard_map/all_to_all | solution.py:35
  173.0 110.3 %all-gather.6.cloned.1.call-start = ((), (), s32[]{:S(2)}) async-start(), calls=%async_computation.6 | async-start | bytes 6684672 | tf_op jit(solution)/shard_map/all_gather | solution.py:211
  241.2 122.4 %reduce-scatter.2.cloned.1.call-start = ((), (), s32[]{:S(2)}) async-start(), calls=%async_computation.5 | async-start | bytes 6684672 | tf_op jit(solution)/shard_map/reduce_scatter | solution.py:214
  283.3 5.8 %copy-start.5 = (bf16[2,2048,256]{2,1,0:T(8,128)(2,1)S(1)}, bf16[2,2048,256]{2,1,0:T(8,128)(2,1)}, u32[]{:S(2)}) copy-start(bf16[2,2048,256]{2,1,0:T(8,128)(2,1)} %param.35) | copy-start | bytes 6291460
  289.1 1.8 copy-start.6
Sparse Core Ops, SparseCore 0:
  17.3 77.1 all-gather.3
  241.3 41.9 all-gather.5
  297.8 65.6 reduce-scatter.1
where the time goes:
time: 389 us; the launch traced here: 388 us
  waiting for transfers between devices  232 us (60%)
  matrix products  61 us (16%)
  blocking collectives  29.8 us (8%)
  local copies, waits for them, and re-layouts  22.4 us (6%)
  other arithmetic  21.5 us (6%)
  between operations  13.4 us (3%)
  starting transfers between devices  7.47 us (2%)
    all_gather x1, waiting for transfers between devices, in_one_piece(): lax.all_gather(both, axis, axis=dim, tiled=True)  77.3 us
    reduce_scatter x1, waiting for transfers between devices, body(): lax.psum_scatter(jnp.einsum('secf,efd->secd', flat_hidden, down_weight, p...  65.9 us
    all_to_all x1, waiting for transfers between devices, sum_at_owner(): lax.all_to_all(tiles, axis, split_axis=0, concat_axis=0, tiled=True)  47.3 us
    all_gather x1, waiting for transfers between devices, body(): lax.all_gather(arrived[None], 'tp', axis=0, tiled=True)  41.8 us
    dot_general x2, matrix products, fold_group(): jnp.einsum('qhr,kr->qhk', queries[..., nope:], key_turned, preferred_elem...  18.8 us
    all_to_all x1, blocking collectives, body(): lax.all_to_all(summed, 'sp', split_axis=0, concat_axis=0, tiled=True)  15.1 us
    all_to_all x1, blocking collectives, body(): lax.all_to_all(outgoing, 'sp', split_axis=0, concat_axis=0, tiled=True)  14.7 us
    dot_general x2, matrix products, fold_group(): jnp.einsum('qhk,khd->qhd', weights.astype(jnp.bfloat16), value_rows, pref...  14.1 us
  transfers between devices with their start and end apart: 4, of which 4 were waited for; matrix products, arithmetic and copies ran while one was open for 0% of the time, Pallas kernels for 0%

commit v1 on v0

v1 whole, which is shorter than its diff:
```python
import jax
import jax.numpy as jnp
from jax import lax
from jax.experimental import pallas as pl
from jax.experimental.pallas import tpu as pltpu
from jax.sharding import PartitionSpec as P

NA, NB, ROPE, CAP = 64, 128, 32, 3
EPS = 1e-6
MASKED = -1e30
LOG2E = 1.4426950408889634
SIDE = 4
HALF_ROWS = 256
KT_ROWS = 16
PIECE = HALF_ROWS + KT_ROWS
CUT = 144
MESH_ID = pl.DeviceIdType.MESH
STEPS = (
    (-1, 0), (1, 0), (0, -1), (0, 1), (2, 0), (-1, -1), (-1, 1), (1, -1), (1, 1),
    (0, 2), (2, -1), (2, 1), (-1, 2), (1, 2), (2, 2),
)


def pick(index, values):
    out = jnp.int32(values[0])
    for at, value in enumerate(values):
        if at:
            out = jnp.where(index == at, jnp.int32(value), out)
    return out


def attend_kernel(
    own, q1, q2, wup, of_hbm, os_hbm, res_hbm, gain,
    mid_ref, norm_ref,
    buf, wout, res, m1, l1, o1, m2, l2, o2, att, po, px, pd, rs_out, rs_in,
    g_send, g_recv, d_send, d_recv, loc_sem, x_send, x_recv, r_send, r_recv,
):
    me = lax.axis_index("sp")
    tp = lax.axis_index("tp")
    core = lax.rem(tp, 2)
    z = lax.div(tp, 2)
    y = lax.div(me, SIDE)
    x = lax.rem(me, SIDE)
    zn = lax.axis_size("tp") // 2

    def block(c, dp, dq):
        p = lax.rem(x + c * (y - x) + dp + SIDE, SIDE)
        q = lax.rem(y + c * (x - y) + dq + SIDE, SIDE)
        return p * (1 + 3 * c) + q * (4 - 3 * c)

    def sp_dev(dp, dq):
        return {"sp": block(core, dp, dq), "tp": tp}

    sib = {"sp": me, "tp": tp + 1 - 2 * core}
    z_up = {"sp": me, "tp": lax.rem(z + 1, zn) * 2 + core}
    z_dn = {"sp": me, "tp": lax.rem(z + zn - 1, zn) * 2 + core}
    peers = [sp_dev(1, 0), sp_dev(-1, 0), sp_dev(0, 1), sp_dev(0, -1), sib, z_up, z_dn]

    loads = [
        pltpu.make_async_copy(of_hbm, wout.at[pl.ds(64, 64)], loc_sem.at[0]),
        pltpu.make_async_copy(os_hbm, wout.at[pl.ds(128, 128)], loc_sem.at[1]),
        pltpu.make_async_copy(res_hbm.at[pl.ds(pl.multiple_of(tp * 32, 32), 32)], res, loc_sem.at[2]),
    ]
    for load in loads:
        load.start()
    wout[pl.ds(0, 64)] = jnp.zeros((64, wout.shape[1]), wout.dtype)

    barrier = pltpu.get_barrier_semaphore()
    for peer in peers:
        pl.semaphore_signal(barrier, inc=1, device_id=peer, device_id_type=MESH_ID)
    pl.semaphore_wait(barrier, len(peers))

    A, B, FULL = (0, CUT), (CUT, PIECE - CUT), (0, PIECE)

    def g_copy(sem, off, rows, dev, src_own=False):
        b = block(core, *off)
        src = own.at[core, pl.ds(rows[0], rows[1])] if src_own else buf.at[b, core, pl.ds(rows[0], rows[1])]
        return pltpu.make_async_remote_copy(
            src_ref=src, dst_ref=buf.at[b, core, pl.ds(rows[0], rows[1])],
            send_sem=g_send.at[sem], recv_sem=g_recv.at[sem],
            device_id=dev, device_id_type=MESH_ID,
        )

    right, left, up, down = sp_dev(1, 0), sp_dev(-1, 0), sp_dev(0, 1), sp_dev(0, -1)
    X, L, R, O = (0, 0), (-1, 0), (1, 0), (2, 0)
    sends = {
        0: (X, FULL, right, True), 1: (X, FULL, left, True), 2: (X, FULL, up, True), 3: (X, FULL, down, True),
        4: (L, A, right, False), 5: (R, B, left, False),
        6: (L, FULL, up, False), 7: (L, FULL, down, False), 8: (R, FULL, up, False), 9: (R, FULL, down, False),
        10: (O, FULL, up, False), 11: (O, FULL, down, False),
    }
    for k, dp in enumerate((0, -1, 1, 2)):
        sends[12 + 2 * k] = ((dp, -1), A, up, False)
        sends[13 + 2 * k] = ((dp, 1), B, down, False)
    arrive = {0: (L, FULL), 1: (R, FULL), 2: ((0, -1), FULL), 3: ((0, 1), FULL), 4: (O, A), 5: (O, B)}
    for k, dp in enumerate((0, -1, 1, 2)):
        if k:
            arrive[4 + 2 * k] = ((dp, -1), FULL)
            arrive[5 + 2 * k] = ((dp, 1), FULL)
        arrive[12 + 2 * k] = ((dp, 2), A)
        arrive[13 + 2 * k] = ((dp, 2), B)

    def send(sem):
        off, rows, dev, src_own = sends[sem]
        g_copy(sem, off, rows, dev, src_own).start()

    def arrived(sem):
        off, rows = arrive[sem]
        g_copy(sem, off, rows, right).wait_recv()

    def d_copy(event, blk, half):
        return pltpu.make_async_remote_copy(
            src_ref=buf.at[blk, half], dst_ref=buf.at[blk, half],
            send_sem=d_send.at[event], recv_sem=d_recv.at[event],
            device_id=sib, device_id_type=MESH_ID,
        )

    events = [
        ((0,), (4, 6, 7)), ((1,), (5, 8, 9)), ((2,), (12,)), ((3,), (13,)), ((4, 5), (10, 11)),
        ((6,), (14,)), ((7,), (15,)), ((8,), (16,)), ((9,), (17,)),
        ((12, 13), ()), ((10,), (18,)), ((11,), (19,)), ((14, 15), ()), ((16, 17), ()), ((18, 19), ()),
    ]

    for sem in (0, 1, 2, 3):
        send(sem)

    c1 = LOG2E * (NA + ROPE) ** -0.5
    c2 = LOG2E * (NB + ROPE) ** -0.5
    m1[...] = jnp.full(m1.shape, MASKED, jnp.float32)
    m2[...] = jnp.full(m2.shape, MASKED, jnp.float32)
    for ref in (l1, o1, l2, o2):
        ref[...] = jnp.zeros(ref.shape, jnp.float32)

    def unpack_turned(packed):
        wide = packed.astype(jnp.float32)
        rolled = [wide] + [pltpu.roll(wide, 512 - 32 * j, 1) for j in (1, 2, 3)]
        parts = [rolled[k % 4][:, (k // 4) * 128:(k // 4) * 128 + 128] for k in range(16)]
        return jnp.concatenate(parts, axis=0).astype(jnp.bfloat16)

    def head(q, keys, values, m, l, o, scale, masked):
        s = lax.dot_general(q[...], keys, (((1,), (1,)), ((), ())), preferred_element_type=jnp.float32)
        if masked is not None:
            s = jnp.where(masked, s, MASKED)
        old = m[...]
        new = jnp.maximum(old, jnp.max(s, axis=1, keepdims=True))
        m[...] = new
        fade = jnp.exp2((old - new) * scale)
        p = jnp.exp2((s - jnp.concatenate([new, new], axis=1)) * scale)
        l[...] = l[...] * fade + (p[:, :128] + p[:, 128:])
        o[...] = o[...] * fade + jnp.dot(p.astype(jnp.bfloat16), values, preferred_element_type=jnp.float32)

    def compute(piece, masked):
        turned = unpack_turned(piece[pl.ds(0, KT_ROWS)])
        kv = jnp.dot(piece[pl.ds(KT_ROWS, HALF_ROWS)], wup[...], preferred_element_type=jnp.float32).astype(jnp.bfloat16)
        kfv = kv[:, 128:256]
        head(q1, jnp.concatenate([kfv, turned], axis=1), kfv, m1, l1, o1, c1, masked)
        head(q2, jnp.concatenate([kv[:, :128], turned], axis=1), kv[:, 256:384], m2, l2, o2, c2, masked)

    def diag(half, _):
        rows = lax.broadcasted_iota(jnp.int32, (2 * HALF_ROWS, HALF_ROWS), 0)
        cols = lax.broadcasted_iota(jnp.int32, (2 * HALF_ROWS, HALF_ROWS), 1) + half * HALF_ROWS
        compute(own.at[half], rows >= cols)
        return 0

    lax.fori_loop(0, 2, diag, 0)

    def step(it, _):
        event = lax.div(it, 2)
        theirs = lax.rem(it, 2)
        stream = core + theirs * (1 - 2 * core)
        blk = block(stream, pick(event, [s[0] for s in STEPS]), pick(event, [s[1] for s in STEPS]))

        for number, (waits, starts) in enumerate(events):
            @pl.when(it == 2 * number)
            def _():
                for sem in waits:
                    arrived(sem)
                for sem in starts:
                    send(sem)

        @pl.when(theirs == 0)
        def _():
            d_copy(event, blk, core).start()

        @pl.when(theirs == 1)
        def _():
            d_copy(event, blk, 1 - core).wait_recv()

        @pl.when(blk < me)
        def _():
            compute(buf.at[blk, stream], None)

        return 0

    lax.fori_loop(0, 2 * len(events), step, 0)

    for sem in range(20):
        off, rows, dev, src_own = sends[sem]
        g_copy(sem, off, rows, dev, src_own).wait_send()

    def drain(event, _):
        d_copy(event, block(core, pick(event, [s[0] for s in STEPS]), pick(event, [s[1] for s in STEPS])), core).wait_send()
        return 0

    lax.fori_loop(0, len(events), drain, 0)

    a1 = o1[...] / jnp.sum(l1[...], axis=1, keepdims=True)
    a2 = o2[...] / jnp.sum(l2[...], axis=1, keepdims=True)
    lane = lax.broadcasted_iota(jnp.int32, a1.shape, 1)
    a1 = jnp.where(lane >= 64, a1, 0.0)
    both = jnp.concatenate([a1, a2], axis=1).astype(jnp.bfloat16)
    att[...] = both.reshape(att.shape)

    for load in loads:
        load.wait()

    def project(c, into):
        rows = att[:, pl.ds(c, 1)].reshape(zn * 32, 256)
        into[...] = jnp.dot(rows, wout[...], preferred_element_type=jnp.float32).astype(jnp.bfloat16).reshape(into.shape)

    def x_copy(d):
        at = lax.rem(z + d, zn)
        return pltpu.make_async_remote_copy(
            src_ref=px.at[at], dst_ref=pd.at[at], send_sem=x_send.at[d], recv_sem=x_recv.at[d],
            device_id=sib, device_id_type=MESH_ID,
        )

    far = zn // 2
    order = [far]
    for d in range(far - 1, 0, -1):
        order += [d, zn - d]
    order.append(0)
    project(1 - core, px)
    for d in order:
        x_copy(d).start()
    project(core, po)

    halves = (0, 1024)

    def pair_sum(at, col, width):
        return po[at, :, pl.ds(col, width)].astype(jnp.float32) + pd[at, :, pl.ds(col, width)].astype(jnp.float32)

    def r_copy(direction, hop, part):
        return pltpu.make_async_remote_copy(
            src_ref=rs_out.at[direction, hop, part], dst_ref=rs_in.at[direction, hop, part],
            send_sem=r_send.at[direction, hop, part], recv_sem=r_recv.at[direction, hop, part],
            device_id=z_up if direction == 0 else z_dn, device_id_type=MESH_ID,
        )

    seen = set()

    def ring(direction, hop, part):
        d = far - hop
        shift = d if direction == 0 else (zn - d) % zn
        if shift not in seen:
            x_copy(shift).wait_recv()
            seen.add(shift)
        total = pair_sum(lax.rem(z + shift, zn), halves[part], 1024)
        if hop > 0 and not (hop == 1 and part != direction):
            r_copy(direction, hop - 1, part).wait_recv()
            total = total + rs_in[direction, hop - 1, part].astype(jnp.float32)
        rs_out[direction, hop, part] = total.astype(jnp.bfloat16)
        r_copy(direction, hop, part).start()

    used = []
    for hop, flip in ((0, 0), (1, 1), (1, 0), (2, 1), (2, 0), (3, 1), (3, 0)):
        for direction in (0, 1):
            part = direction if flip == 0 else 1 - direction
            ring(direction, hop, part)
            used.append((direction, hop, part))
    x_copy(0).wait_recv()
    mids = []
    for part in (0, 1):
        total = pair_sum(z, halves[part], 1024)
        for direction in (0, 1):
            r_copy(direction, far - 1, part).wait_recv()
            total = total + rs_in[direction, far - 1, part].astype(jnp.float32)
        mids.append((res[:, pl.ds(halves[part], 1024)].astype(jnp.float32) + total).astype(jnp.bfloat16))
    mid = jnp.concatenate(mids, axis=1)
    mid_ref[...] = mid
    wide = mid.astype(jnp.float32)
    norm_ref[...] = (wide * lax.rsqrt(jnp.mean(wide * wide, axis=1, keepdims=True) + EPS) * gain[...]).astype(jnp.bfloat16)
    for d in order:
        x_copy(d).wait_send()
    for item in used:
        r_copy(*item).wait_send()


def attend(own, q1, q2, wup, out_first, out_second, residual, gain):
    vmem = pl.BlockSpec(memory_space=pltpu.VMEM)
    hbm = pl.BlockSpec(memory_space=pl.ANY)
    f32, bf16 = jnp.float32, jnp.bfloat16
    dma = pltpu.SemaphoreType.DMA
    row = pltpu.VMEM((512, 128), f32)
    return pl.pallas_call(
        attend_kernel,
        out_shape=[jax.ShapeDtypeStruct((32, 2048), bf16)] * 2,
        in_specs=[vmem, vmem, vmem, vmem, hbm, hbm, hbm, vmem],
        out_specs=[vmem, vmem],
        scratch_shapes=[
            pltpu.VMEM((16, 2, PIECE, 512), bf16),
            pltpu.VMEM((256, 2048), bf16),
            pltpu.VMEM((32, 2048), bf16),
            row, row, row, row, row, row,
            pltpu.VMEM((8, 2, 32, 256), bf16),
            pltpu.VMEM((8, 32, 2048), bf16),
            pltpu.VMEM((8, 32, 2048), bf16),
            pltpu.VMEM((8, 32, 2048), bf16),
            pltpu.VMEM((2, 4, 2, 32, 1024), bf16),
            pltpu.VMEM((2, 4, 2, 32, 1024), bf16),
            dma((20,)), dma((20,)), dma((15,)), dma((15,)), dma((3,)),
            dma((8,)), dma((8,)), dma((2, 4, 2)), dma((2, 4, 2)),
        ],
        compiler_params=pltpu.CompilerParams(collective_id=1, has_side_effects=True, vmem_limit_bytes=48 * 2**20),
        name="gather_attend",
    )(own, q1, q2, wup, out_first, out_second, residual, gain)


def rotate(values, positions):
    half = values.shape[-1] // 2
    inverse = 10000.0 ** (-jnp.arange(half, dtype=jnp.float32) / half)
    angles = positions.astype(jnp.float32)[:, None] * inverse[None, :]
    cosine = jnp.cos(angles)
    sine = jnp.sin(angles)
    first = values[:, :half]
    second = values[:, half:]
    return jnp.concatenate([first * cosine - second * sine, second * cosine + first * sine], axis=-1)


def rms_scaled(values, gain):
    wide = values.astype(jnp.float32)
    return wide * lax.rsqrt(jnp.mean(wide * wide, axis=-1, keepdims=True) + EPS) * gain


def turned(query, nope, places):
    rows = query.shape[0]
    rot = rotate(query[:, nope:].astype(jnp.float32), places).astype(jnp.bfloat16)
    pieces = [query[:, :nope]]
    if nope < 128:
        pieces.append(jnp.zeros((rows, 128 - nope), jnp.bfloat16))
    pieces += [rot, jnp.zeros((rows, 128 - ROPE), jnp.bfloat16)]
    return jnp.concatenate(pieces, axis=-1)


def attention_part(
    query_first, query_second, latent, key_rotary, latent_gain, key_up_first, value_up_first,
    key_up_second, value_up_second, out_first, out_second, residual, expert_gain,
):
    rows = latent.shape[0]
    places = lax.axis_index("sp") * rows + jnp.arange(rows, dtype=jnp.int32)
    q1 = turned(query_first, NA, places)
    q2 = turned(query_second, NB, places)
    key_turned = rotate(key_rotary.astype(jnp.float32), places).astype(jnp.bfloat16)
    normed = rms_scaled(latent, latent_gain).astype(jnp.bfloat16)
    packed = key_turned.reshape(2, 16, 16, ROPE).transpose(0, 2, 1, 3).reshape(2, KT_ROWS, 512)
    own = jnp.concatenate([packed, normed.reshape(2, HALF_ROWS, 512)], axis=1)
    wup = jnp.concatenate([key_up_second, key_up_first, value_up_first, value_up_second], axis=1)
    return attend(own, q1, q2, wup, out_first, out_second, residual, expert_gain.reshape(1, -1))


def clamped_unit(gate, upward):
    limited = jnp.minimum(gate, 7.0)
    bounded = jnp.clip(upward, -7.0, 7.0)
    return (bounded + 1.0) * limited * jax.nn.sigmoid(1.702 * limited)


def slot_numbers(chosen, experts):
    hits = (chosen[..., None] == jnp.arange(experts, dtype=jnp.int32)).astype(jnp.int32)
    before = jnp.cumsum(hits, axis=-2) - hits
    return chosen * CAP + jnp.sum(before * hits, axis=-1)


def expert_hidden(rows, gate_weight, up_weight):
    gate = jnp.einsum("nsecd,edf->nsecf", rows, gate_weight, preferred_element_type=jnp.float32)
    upward = jnp.einsum("nsecd,edf->nsecf", rows, up_weight, preferred_element_type=jnp.float32)
    return clamped_unit(gate, upward).astype(jnp.bfloat16)


def body(
    query_first, query_second, latent, key_rotary, latent_gain, key_up_first, value_up_first,
    key_up_second, value_up_second, out_first, out_second, residual, expert_gain,
    route_experts, route_scores, gate_weight, up_weight, down_weight,
):
    middle, normed = attention_part(
        query_first, query_second, latent, key_rotary, latent_gain, key_up_first, value_up_first,
        key_up_second, value_up_second, out_first, out_second, residual, expert_gain,
    )
    sets = lax.axis_size("tp")
    groups = lax.axis_size("sp")
    own_rows = latent.shape[0] // sets
    topk = route_experts.shape[1]
    local_experts = gate_weight.shape[0]
    experts = local_experts * groups
    own_start = lax.axis_index("tp") * own_rows
    slot_range = jnp.arange(experts * CAP, dtype=jnp.int32)
    own_ids = lax.dynamic_slice_in_dim(route_experts, own_start, own_rows, 0).reshape(-1)
    own_slots = slot_numbers(own_ids, experts)
    picks = (own_slots[:, None] == slot_range).reshape(own_rows, topk, experts * CAP)
    selected = jnp.sum(picks.astype(jnp.float32), axis=1).astype(jnp.bfloat16)
    outgoing = jnp.einsum("ts,td->sd", selected, normed, preferred_element_type=jnp.float32).astype(jnp.bfloat16)
    outgoing = outgoing.reshape(groups, local_experts, CAP, outgoing.shape[-1])
    arrived = lax.all_to_all(outgoing, "sp", split_axis=0, concat_axis=0, tiled=True)
    activated = expert_hidden(lax.all_gather(arrived[None], "tp", axis=0, tiled=True), gate_weight, up_weight)
    flat_hidden = activated.reshape(sets * groups, local_experts, CAP, activated.shape[-1])
    summed = lax.psum_scatter(
        jnp.einsum("secf,efd->secd", flat_hidden, down_weight, preferred_element_type=jnp.float32).astype(jnp.bfloat16),
        "tp", scatter_dimension=0, tiled=True,
    )
    returned = lax.all_to_all(summed, "sp", split_axis=0, concat_axis=0, tiled=True)
    expert_out = returned.reshape(experts * CAP, returned.shape[-1]).astype(jnp.float32)
    own_scores = lax.dynamic_slice_in_dim(route_scores, own_start, own_rows, 0)
    route_weight = jax.nn.softmax(own_scores, axis=-1)
    matches = own_slots.reshape(own_rows, topk)[..., None] == slot_range
    combine = jnp.sum(jnp.where(matches, route_weight[..., None], 0.0), axis=1)
    mixture = jnp.dot(combine, expert_out)
    return (middle.astype(jnp.float32) + mixture).astype(jnp.bfloat16)


def solution(mesh):
    in_specs = (
        P("sp", "tp"), P("sp", "tp"), P("sp", None), P("sp", None), P(),
        P(None, "tp"), P(None, "tp"), P(None, "tp"), P(None, "tp"),
        P("tp", None), P("tp", None), P("sp", None), P(),
        P("sp", None), P("sp", None), P("sp", None, "tp"), P("sp", None, "tp"), P("sp", "tp", None),
    )
    out_specs = P(("sp", "tp"), None)
    return jax.shard_map(body, mesh=mesh, in_specs=in_specs, out_specs=out_specs, check_vma=False)
```

time: 389 us -> 262 us (0.67)
  waiting for transfers between devices: 232 us -> 108 us
  Pallas kernels: 0 us -> 62.8 us
  matrix products: 61 us -> 9.56 us
  other arithmetic: 21.5 us -> 8.61 us
  starting transfers between devices: 7.47 us -> 0.22 us
  blocking collectives: 29.8 us -> 34.4 us
    all_gather x1 -> x0, waiting for transfers between devices: 77.3 us -> none  [in_one_piece(): lax.all_gather(both, axis, axis=dim, tiled=True)]
    pallas_call x0 -> x1, Pallas kernels: none -> 62.8 us  [attend(): pl.pallas_call(attend_kernel, out_shape=[jax.ShapeDtypeStruct((32, 2048),...]
    dot_general x12 -> x0, matrix products: 51.4 us -> none  [the longest x2 18.8 us: fold_group(): jnp.einsum('qhr,kr->qhk', queries[..., nope:], key_turned, preferred_elem...]
    all_to_all x1 -> x0, waiting for transfers between devices: 47.3 us -> none  [sum_at_owner(): lax.all_to_all(tiles, axis, split_axis=0, concat_axis=0, tiled=True)]
    reduce_sum x4 -> x1, other arithmetic: 18.3 us -> 1.22 us  [rms_scaled(): jnp.mean(wide * wide, axis=-1, keepdims=True) + EPS]
    another operation x2 -> x1, local copies, waits for them, and re-layouts: 11.8 us -> 0.02 us
    all_to_all x1 -> x0, starting transfers between devices: 7.17 us -> none  [sum_at_owner(): lax.all_to_all(tiles, axis, split_axis=0, concat_axis=0, tiled=True)]
    unnamed x13 -> x36, local copies, waits for them, and re-layouts: 0.86 us -> 7.69 us
  transfers between devices with their start and end apart: 4 -> 2, of which waited for: 4 -> 2; matrix products, arithmetic and copies ran while one was open for 0% -> 0% of each run, Pallas kernels for 0% -> 0%
where the time goes in v1:
time: 262 us
  waiting for transfers between devices  108 us (41%)
  Pallas kernels  62.8 us (24%)
  blocking collectives  34.4 us (13%)
  local copies, waits for them, and re-layouts  24.3 us (9%)
  between operations  13.7 us (5%)
  matrix products  9.56 us (4%)
  other arithmetic  8.61 us (3%)
    reduce_scatter x1, waiting for transfers between devices, body(): lax.psum_scatter(jnp.einsum('secf,efd->secd', flat_hidden, down_weight, p...  65.9 us
    pallas_call x1, Pallas kernels, attend(): pl.pallas_call(attend_kernel, out_shape=[jax.ShapeDtypeStruct((32, 2048),...  62.8 us
    all_gather x1, waiting for transfers between devices, body(): lax.all_gather(arrived[None], 'tp', axis=0, tiled=True)  42.1 us
    all_to_all x1, blocking collectives, body(): lax.all_to_all(outgoing, 'sp', split_axis=0, concat_axis=0, tiled=True)  19.3 us
    all_to_all x1, blocking collectives, body(): lax.all_to_all(summed, 'sp', split_axis=0, concat_axis=0, tiled=True)  15.1 us
    unnamed x36, local copies, waits for them, and re-layouts  7.69 us
    all_gather x1, local copies, waits for them, and re-layouts, body(): lax.all_gather(arrived[None], 'tp', axis=0, tiled=True)  5.83 us
  transfers between devices with their start and end apart: 2, of which 2 were waited for; matrix products, arithmetic and copies ran while one was open for 0% of the time, Pallas kernels for 0%

profile of v1, /device:TPU:2, one launch (start us, length us, event | category | flops | bytes accessed | tf_op | source)
XLA Modules:
  0.0 261.7 jit_solution(12902359909211727348)
XLA Ops:
  6.6 0.9 slice.33
  7.5 0.8 slice.32
  9.1 1.6 slice.36
  13.7 1.2 fusion.17
  17.0 2.0 fusion.41
  19.6 1.7 copy.117
  21.6 1.1 pad_maximum_fusion.1.wup
  22.7 1.1 pad_maximum_fusion.2.q2
  24.5 2.0 concatenate.31.q1
  26.5 1.6 copy-done.1
  28.1 0.9 copy-done.2
  29.1 1.0 copy-done.3
  30.1 0.9 copy-done.4
  31.1 62.8 %gather_attend.1 = (bf16[32,2048]{1,0:T(8,128)(2,1)S(1)}, bf16[32,2048]{1,0:T(8,128)(2,1)S(1)}) custom-call(bf16[2,272,512]{2,1,0:T(8,128)(2,1)S(1)} %pad_maximum_fusion.own, bf16[512,256]{1,0:T(8,128)(2,1)S(1)} %copy-done.2, bf16[512,256]{1,0:T(8,128)(2,1)S(1)} %pad_maximum_fusion.2.q2, bf16[512,384]{1,0:T(8,128)(2,1)S(1)} %pad_maximum_fusion.1.wup, ...), custom_call_target="tpu_custom_call" | custom-call | tf_op jit(solution)/shard_map/gather_attend/pallas_call | solution.py:295
  94.9 19.3 %all_to_all.10 = bf16[16,2,3,2048]{3,1,2,0:T(2,128)(2,1)} all-to-all(bf16[16,2,3,2048]{3,1,2,0:T(2,128)(2,1)S(1)} %copy.105), channel_id=1, replica_groups=mesh['sp'=16,'tp'=16] {'sp'}, dimensions={0} | all-to-all | bytes 786432 | tf_op jit(solution)/shard_map/all_to_all | solution.py:402
  114.4 42.1 %all-gather.3.cloned.1.call-done = bf16[256,2,3,2048]{3,1,2,0:T(2,128)(2,1)} async-done(((bf16[16,2,3,2048]{3,1,2,0:T(2,128)(2,1)}), bf16[256,2,3,2048]{3,1,2,0:T(2,128)(2,1)}) %all-gather.3.cloned.1.call-update) | async-done | bytes 6291472 | tf_op jit(solution)/shard_map/all_gather | solution.py:403
  156.6 5.8 %copy.106 = bf16[256,2,3,2048]{3,0,2,1:T(8,128)(2,1)S(1)} copy(bf16[256,2,3,2048]{3,1,2,0:T(2,128)(2,1)} %all-gather.3.cloned.1.call-done) | data formatting | bytes 12582912 | tf_op jit(solution)/shard_map/all_gather | solution.py:403
  162.4 1.8 fusion
  164.2 2.2 fusion.12
  166.5 4.5 %convert_bitcast_fusion = bf16[256,2,3,2048]{3,0,2,1:T(8,128)(2,1)} fusion(bf16[256,2,3,256]{3,0,2,1:T(8,128)(2,1)S(1)} %bitcast.41, bf16[2,256,2048]{2,1,0:T(8,128)(2,1)S(1)} %copy-done), kind=kOutput, calls=%fused_computation | convolution fusion | flops 1613758464 | bytes 9175040 | tf_op jit(solution)/shard_map/secf,efd->secd/dot_general | solution.py:406
  171.0 65.9 %reduce-scatter.2.cloned.1.call-done = bf16[16,2,3,2048]{3,0,2,1:T(8,128)(2,1)} async-done(((bf16[256,2,3,2048]{3,0,2,1:T(8,128)(2,1)}), bf16[16,2,3,2048]{3,0,2,1:T(8,128)(2,1)}) %reduce-scatter.2.cloned.1.call-update) | async-done | bytes 393232 | tf_op jit(solution)/shard_map/reduce_scatter | solution.py:405
  236.8 1.4 copy.110
  238.2 15.1 %all_to_all.11 = bf16[16,2,3,2048]{3,1,2,0:T(2,128)(2,1)S(1)} all-to-all(bf16[16,2,3,2048]{3,1,2,0:T(2,128)(2,1)S(1)} %copy.110), channel_id=1, replica_groups=mesh['sp'=16,'tp'=16] {'sp'}, dimensions={0} | all-to-all | bytes 786432 | tf_op jit(solution)/shard_map/all_to_all | solution.py:409
  254.0 0.8 fusion.4
  (67 shorter events, 9.3 us)
Async XLA Ops:
  6.5 159.9 %copy-start = (bf16[2,256,2048]{2,1,0:T(8,128)(2,1)S(1)}, bf16[2,256,2048]{2,1,0:T(8,128)(2,1)}, u32[]{:S(2)}) copy-start(bf16[2,256,2048]{2,1,0:T(8,128)(2,1)} %param.35) | copy-start | bytes 6291460
  6.5 10.2 %copy-start.10 = (bf16[512,32]{0,1:T(8,128)(2,1)S(1)}, bf16[512,32]{0,1:T(8,128)(2,1)}, u32[]{:S(2)}) copy-start(bf16[512,32]{0,1:T(8,128)(2,1)} %param.21) | copy-start | bytes 98308
  6.5 150.0 %all-gather.3.cloned.1.call-start = ((), (), s32[]{:S(2)}) async-start(), calls=%async_computation.4 | async-start | bytes 6684672 | tf_op jit(solution)/shard_map/all_gather | solution.py:403
  16.7 2.6 copy-start.8
  16.7 2.7 %copy-start.9 = (bf16[512,64]{0,1:T(8,128)(2,1)S(1)}, bf16[512,64]{0,1:T(8,128)(2,1)}, u32[]{:S(2)}) copy-start(bf16[512,64]{0,1:T(8,128)(2,1)} %param.24) | copy-start | bytes 196612
  16.9 4.4 %copy-start.6 = (bf16[512,512]{1,0:T(8,128)(2,1)S(1)}, bf16[512,512]{1,0:T(8,128)(2,1)}, u32[]{:S(2)}) copy-start(bf16[512,512]{1,0:T(8,128)(2,1)} %param.20) | copy-start | bytes 1572868
  16.9 4.4 %copy-start.11 = (f32[512]{0:T(512)S(1)}, f32[512]{0:T(512)}, u32[]{:S(2)}) copy-start(f32[512]{0:T(512)} %param.22) | copy-start | bytes 6148
  21.2 1.5 copy-start.7
  21.5 5.0 %copy-start.5 = (f32[2048]{0:T(1024)S(1)}, f32[2048]{0:T(1024)}, u32[]{:S(2)}) copy-start(f32[2048]{0:T(1024)} %param.30) | copy-start | bytes 24580
  26.5 1.6 copy-start.1
  28.1 0.9 copy-start.2
  29.1 1.0 copy-start.3
  30.1 0.9 copy-start.4
  114.2 122.7 %reduce-scatter.2.cloned.1.call-start = ((), (), s32[]{:S(2)}) async-start(), calls=%async_computation.3 | async-start | bytes 6684672 | tf_op jit(solution)/shard_map/reduce_scatter | solution.py:405
  156.6 5.8 %copy-start.12 = (bf16[2,2048,256]{2,1,0:T(8,128)(2,1)S(1)}, bf16[2,2048,256]{2,1,0:T(8,128)(2,1)}, u32[]{:S(2)}) copy-start(bf16[2,2048,256]{2,1,0:T(8,128)(2,1)} %param.33) | copy-start | bytes 6291460
  162.4 1.8 copy-start.13
Sparse Core Ops, SparseCore 0:
  114.3 42.2 all-gather.2
  171.1 65.6 reduce-scatter.1

commit v2 on v1

--- a/solution.py
+++ b/solution.py
@@ -1,5 +1,6 @@
 import jax
 import jax.numpy as jnp
+import numpy as np
 from jax import lax
 from jax.experimental import pallas as pl
 from jax.experimental.pallas import tpu as pltpu
@@ -30,8 +31,11 @@
 
 
 def attend_kernel(
-    own, q1, q2, wup, of_hbm, os_hbm, res_hbm, gain,
-    mid_ref, norm_ref,
+    qf_hbm, qs_hbm, lat_hbm, kr_hbm, latg_hbm, kuf_hbm, vuf_hbm, kus_hbm, vus_hbm,
+    of_hbm, os_hbm, res_hbm, gain_hbm, ids_hbm, scores_hbm, base_hbm, start_hbm,
+    mid_ref, out_ref, mix_ref,
+    qf, qs, lat, kr, latg, kuf, vuf, kus, vus, gain, ids, scores, base, start,
+    own, q1, q2, wup,
     buf, wout, res, m1, l1, o1, m2, l2, o2, att, po, px, pd, rs_out, rs_in,
     g_send, g_recv, d_send, d_recv, loc_sem, x_send, x_recv, r_send, r_recv,
 ):
@@ -56,18 +60,67 @@
     z_dn = {"sp": me, "tp": lax.rem(z + zn - 1, zn) * 2 + core}
     peers = [sp_dev(1, 0), sp_dev(-1, 0), sp_dev(0, 1), sp_dev(0, -1), sib, z_up, z_dn]
 
-    loads = [
-        pltpu.make_async_copy(of_hbm, wout.at[pl.ds(64, 64)], loc_sem.at[0]),
-        pltpu.make_async_copy(os_hbm, wout.at[pl.ds(128, 128)], loc_sem.at[1]),
-        pltpu.make_async_copy(res_hbm.at[pl.ds(pl.multiple_of(tp * 32, 32), 32)], res, loc_sem.at[2]),
+    mine = pl.ds(pl.multiple_of(tp * 32, 32), 32)
+    pairs = [
+        (lat_hbm, lat), (latg_hbm, latg), (kr_hbm, kr), (base_hbm, base), (start_hbm, start),
+        (qf_hbm, qf), (qs_hbm, qs), (kus_hbm, kus), (kuf_hbm, kuf), (vuf_hbm, vuf), (vus_hbm, vus),
+        (of_hbm, wout.at[pl.ds(64, 64)]), (os_hbm, wout.at[pl.ds(128, 128)]), (res_hbm.at[mine], res),
+        (gain_hbm, gain), (ids_hbm, ids), (scores_hbm, scores),
     ]
+    loads = [pltpu.make_async_copy(a, b, loc_sem.at[n]) for n, (a, b) in enumerate(pairs)]
     for load in loads:
         load.start()
     wout[pl.ds(0, 64)] = jnp.zeros((64, wout.shape[1]), wout.dtype)
+    m1[...] = jnp.full(m1.shape, MASKED, jnp.float32)
+    m2[...] = jnp.full(m2.shape, MASKED, jnp.float32)
+    for ref in (l1, o1, l2, o2):
+        ref[...] = jnp.zeros(ref.shape, jnp.float32)
 
     barrier = pltpu.get_barrier_semaphore()
     for peer in peers:
         pl.semaphore_signal(barrier, inc=1, device_id=peer, device_id_type=MESH_ID)
+
+    f32, bf16 = jnp.float32, jnp.bfloat16
+
+    def placed(rows, cols, hits):
+        r = lax.broadcasted_iota(jnp.int32, (rows, cols), 0)
+        c = lax.broadcasted_iota(jnp.int32, (rows, cols), 1)
+        total = jnp.zeros((rows, cols), f32)
+        for lo, hi, shift, sign in hits:
+            total = jnp.where((r == c + shift) & (c >= lo) & (c < hi), sign, total)
+        return total.astype(bf16)
+
+    def moved(value, cols, hits):
+        return lax.dot_general(
+            value, placed(value.shape[0], cols, hits), (((0,), (0,)), ((), ())), preferred_element_type=f32
+        )
+
+    for load in loads[:5]:
+        load.wait()
+    cos_r, sin_r = base[0], base[1]
+    cos_0, sin_0 = start[0, pl.ds(me, 1)], start[1, pl.ds(me, 1)]
+    cosine = cos_0 * cos_r - sin_0 * sin_r
+    sine = sin_0 * cos_r + cos_0 * sin_r
+
+    def rot(value, offset):
+        plain = moved(value, 128, [(0, 32, offset, 1.0)])
+        crossed = moved(value, 128, [(0, 16, offset + 16, -1.0), (16, 32, offset - 16, 1.0)])
+        return (plain * cosine + crossed * sine).astype(bf16)
+
+    wide = lat[...].astype(f32)
+    normed = (wide * lax.rsqrt(jnp.mean(wide * wide, axis=1, keepdims=True) + EPS) * latg[...]).astype(bf16)
+    own[:, pl.ds(KT_ROWS, HALF_ROWS)] = normed.reshape(2, HALF_ROWS, 512)
+    kt = rot(kr[...], 0).astype(f32)
+    rolled = [kt] + [pltpu.roll(kt, 32 * j, 1) for j in (1, 2, 3)]
+    for half in (0, 1):
+        tiles = []
+        for tile in range(4):
+            total = 0.0
+            for j in range(4):
+                first = half * HALF_ROWS + (4 * tile + j) * 16
+                total = total + rolled[j][first:first + 16]
+            tiles.append(total)
+        own[half, pl.ds(0, KT_ROWS)] = jnp.concatenate(tiles, axis=1).astype(bf16)
     pl.semaphore_wait(barrier, len(peers))
 
     A, B, FULL = (0, CUT), (CUT, PIECE - CUT), (0, PIECE)
@@ -126,10 +179,15 @@
 
     c1 = LOG2E * (NA + ROPE) ** -0.5
     c2 = LOG2E * (NB + ROPE) ** -0.5
-    m1[...] = jnp.full(m1.shape, MASKED, jnp.float32)
-    m2[...] = jnp.full(m2.shape, MASKED, jnp.float32)
-    for ref in (l1, o1, l2, o2):
-        ref[...] = jnp.zeros(ref.shape, jnp.float32)
+    for load in loads[5:]:
+        load.wait()
+    q1[:, pl.ds(0, 128)] = moved(qf[...], 128, [(0, 64, 0, 1.0)]).astype(bf16)
+    q1[:, pl.ds(128, 128)] = rot(qf[...], NA)
+    q2[:, pl.ds(0, 128)] = moved(qs[...], 128, [(0, 128, 0, 1.0)]).astype(bf16)
+    q2[:, pl.ds(128, 128)] = rot(qs[...], NB)
+    wup[:, pl.ds(0, 128)] = kus[...]
+    wup[:, pl.ds(128, 128)] = (moved(kuf[...], 128, [(0, 64, 0, 1.0)]) + moved(vuf[...], 128, [(64, 128, -64, 1.0)])).astype(bf16)
+    wup[:, pl.ds(256, 128)] = vus[...]
 
     def unpack_turned(packed):
         wide = packed.astype(jnp.float32)
@@ -164,9 +222,11 @@
 
     lax.fori_loop(0, 2, diag, 0)
 
+    count = len(events)
+
     def step(it, _):
-        event = lax.div(it, 2)
         theirs = lax.rem(it, 2)
+        event = lax.div(it, 2) - theirs
         stream = core + theirs * (1 - 2 * core)
         blk = block(stream, pick(event, [s[0] for s in STEPS]), pick(event, [s[1] for s in STEPS]))
 
@@ -178,21 +238,21 @@
                 for sem in starts:
                     send(sem)
 
-        @pl.when(theirs == 0)
+        @pl.when((theirs == 0) & (event < count))
         def _():
             d_copy(event, blk, core).start()
 
-        @pl.when(theirs == 1)
+        @pl.when((theirs == 1) & (event >= 0))
         def _():
             d_copy(event, blk, 1 - core).wait_recv()
 
-        @pl.when(blk < me)
+        @pl.when((blk < me) & (event >= 0) & (event < count))
         def _():
             compute(buf.at[blk, stream], None)
 
         return 0
 
-    lax.fori_loop(0, 2 * len(events), step, 0)
+    lax.fori_loop(0, 2 * count + 2, step, 0)
 
     for sem in range(20):
         off, rows, dev, src_own = sends[sem]
@@ -202,7 +262,7 @@
         d_copy(event, block(core, pick(event, [s[0] for s in STEPS]), pick(event, [s[1] for s in STEPS])), core).wait_send()
         return 0
 
-    lax.fori_loop(0, len(events), drain, 0)
+    lax.fori_loop(0, count, drain, 0)
 
     a1 = o1[...] / jnp.sum(l1[...], axis=1, keepdims=True)
     a2 = o2[...] / jnp.sum(l2[...], axis=1, keepdims=True)
@@ -211,8 +271,6 @@
     both = jnp.concatenate([a1, a2], axis=1).astype(jnp.bfloat16)
     att[...] = both.reshape(att.shape)
 
-    for load in loads:
-        load.wait()
 
     def project(c, into):
         rows = att[:, pl.ds(c, 1)].reshape(zn * 32, 256)
@@ -279,25 +337,63 @@
     mid = jnp.concatenate(mids, axis=1)
     mid_ref[...] = mid
     wide = mid.astype(jnp.float32)
-    norm_ref[...] = (wide * lax.rsqrt(jnp.mean(wide * wide, axis=1, keepdims=True) + EPS) * gain[...]).astype(jnp.bfloat16)
+    normed = (wide * lax.rsqrt(jnp.mean(wide * wide, axis=1, keepdims=True) + EPS) * gain[...]).astype(bf16)
+    slots = out_ref.shape[0]
+    token = lax.broadcasted_iota(jnp.int32, (32, 512), 1) == lax.broadcasted_iota(jnp.int32, (32, 512), 0) + tp * 32
+    names = [jnp.sum(jnp.where(token, ids[k:k + 1], 0), axis=1, keepdims=True) for k in (0, 1)]
+    logits = [jnp.sum(jnp.where(token, scores[k:k + 1], 0.0), axis=1, keepdims=True) for k in (0, 1)]
+    hits = [(lax.broadcasted_iota(jnp.int32, (32, 128), 1) == name).astype(f32) for name in names]
+    earlier = lax.broadcasted_iota(jnp.int32, (32, 32), 0) > lax.broadcasted_iota(jnp.int32, (32, 32), 1)
+    before = jnp.dot(earlier.astype(bf16), (hits[0] + hits[1]).astype(bf16), preferred_element_type=f32)
+    top = jnp.maximum(logits[0], logits[1])
+    powers = [jnp.exp(logit - top) for logit in logits]
+    picked, mix = 0.0, 0.0
+    for k in (0, 1):
+        rank = jnp.sum(before * hits[k], axis=1, keepdims=True)
+        slot = names[k] * CAP + rank.astype(jnp.int32)
+        here = (lax.broadcasted_iota(jnp.int32, (32, slots), 1) == slot).astype(f32)
+        picked = picked + here
+        mix = mix + here * (powers[k] / (powers[0] + powers[1]))
+    mix_ref[...] = mix
+    out_ref[...] = lax.dot_general(
+        picked.astype(bf16), normed, (((0,), (0,)), ((), ())), preferred_element_type=f32
+    ).astype(bf16)
     for d in order:
         x_copy(d).wait_send()
     for item in used:
         r_copy(*item).wait_send()
 
 
-def attend(own, q1, q2, wup, out_first, out_second, residual, gain):
+def attend(*args):
+    hbm = pl.BlockSpec(memory_space=pltpu.HBM)
     vmem = pl.BlockSpec(memory_space=pltpu.VMEM)
-    hbm = pl.BlockSpec(memory_space=pl.ANY)
     f32, bf16 = jnp.float32, jnp.bfloat16
     dma = pltpu.SemaphoreType.DMA
     row = pltpu.VMEM((512, 128), f32)
+    place = np.arange(512)[:, None]
+    first = np.arange(16)[:, None] * 512
+    lanes = np.arange(128)[None, :]
+    speed = 10000.0 ** (-(lanes % 16) / 16.0)
+    live = lanes < ROPE
+    base = np.stack([np.cos(place * speed) * live, np.sin(place * speed) * live]).astype(np.float32)
+    start = np.stack([np.cos(first * speed) * live, np.sin(first * speed) * live]).astype(np.float32)
     return pl.pallas_call(
         attend_kernel,
-        out_shape=[jax.ShapeDtypeStruct((32, 2048), bf16)] * 2,
-        in_specs=[vmem, vmem, vmem, vmem, hbm, hbm, hbm, vmem],
-        out_specs=[vmem, vmem],
+        out_shape=[
+            jax.ShapeDtypeStruct((32, 2048), bf16), jax.ShapeDtypeStruct((96, 2048), bf16),
+            jax.ShapeDtypeStruct((32, 96), f32),
+        ],
+        in_specs=[hbm] * 17,
+        out_specs=[vmem] * 3,
         scratch_shapes=[
+            pltpu.VMEM((96, 512), bf16), pltpu.VMEM((160, 512), bf16), pltpu.VMEM((512, 512), bf16),
+            pltpu.VMEM((32, 512), bf16), pltpu.VMEM((1, 512), f32),
+            pltpu.VMEM((64, 512), bf16), pltpu.VMEM((64, 512), bf16),
+            pltpu.VMEM((512, 128), bf16), pltpu.VMEM((512, 128), bf16), pltpu.VMEM((1, 2048), f32),
+            pltpu.VMEM((2, 512), jnp.int32), pltpu.VMEM((2, 512), f32),
+            pltpu.VMEM((2, 512, 128), f32), pltpu.VMEM((2, 16, 128), f32),
+            pltpu.VMEM((2, PIECE, 512), bf16), pltpu.VMEM((512, 256), bf16), pltpu.VMEM((512, 256), bf16),
+            pltpu.VMEM((512, 384), bf16),
             pltpu.VMEM((16, 2, PIECE, 512), bf16),
             pltpu.VMEM((256, 2048), bf16),
             pltpu.VMEM((32, 2048), bf16),
@@ -308,72 +404,201 @@
             pltpu.VMEM((8, 32, 2048), bf16),
             pltpu.VMEM((2, 4, 2, 32, 1024), bf16),
             pltpu.VMEM((2, 4, 2, 32, 1024), bf16),
-            dma((20,)), dma((20,)), dma((15,)), dma((15,)), dma((3,)),
+            dma((20,)), dma((20,)), dma((15,)), dma((15,)), dma((17,)),
             dma((8,)), dma((8,)), dma((2, 4, 2)), dma((2, 4, 2)),
         ],
-        compiler_params=pltpu.CompilerParams(collective_id=1, has_side_effects=True, vmem_limit_bytes=48 * 2**20),
+        compiler_params=pltpu.CompilerParams(collective_id=1, has_side_effects=True, vmem_limit_bytes=67043328),
         name="gather_attend",
-    )(own, q1, q2, wup, out_first, out_second, residual, gain)
-
-
-def rotate(values, positions):
-    half = values.shape[-1] // 2
-    inverse = 10000.0 ** (-jnp.arange(half, dtype=jnp.float32) / half)
-    angles = positions.astype(jnp.float32)[:, None] * inverse[None, :]
-    cosine = jnp.cos(angles)
-    sine = jnp.sin(angles)
-    first = values[:, :half]
-    second = values[:, half:]
-    return jnp.concatenate([first * cosine - second * sine, second * cosine + first * sine], axis=-1)
-
-
-def rms_scaled(values, gain):
-    wide = values.astype(jnp.float32)
-    return wide * lax.rsqrt(jnp.mean(wide * wide, axis=-1, keepdims=True) + EPS) * gain
-
-
-def turned(query, nope, places):
-    rows = query.shape[0]
-    rot = rotate(query[:, nope:].astype(jnp.float32), places).astype(jnp.bfloat16)
-    pieces = [query[:, :nope]]
-    if nope < 128:
-        pieces.append(jnp.zeros((rows, 128 - nope), jnp.bfloat16))
-    pieces += [rot, jnp.zeros((rows, 128 - ROPE), jnp.bfloat16)]
-    return jnp.concatenate(pieces, axis=-1)
-
-
-def attention_part(
-    query_first, query_second, latent, key_rotary, latent_gain, key_up_first, value_up_first,
-    key_up_second, value_up_second, out_first, out_second, residual, expert_gain,
+    )(*args, jnp.asarray(base), jnp.asarray(start))
+
+
+def expert_kernel(
+    own, gate_hbm, up_hbm, down_hbm, out_ref,
+    gx, py, pd, wgu, wdn, rs_out, rs_in,
+    w_sem, g_send, g_recv, s_send, s_recv, x_send, x_recv, r_send, r_recv,
 ):
-    rows = latent.shape[0]
-    places = lax.axis_index("sp") * rows + jnp.arange(rows, dtype=jnp.int32)
-    q1 = turned(query_first, NA, places)
-    q2 = turned(query_second, NB, places)
-    key_turned = rotate(key_rotary.astype(jnp.float32), places).astype(jnp.bfloat16)
-    normed = rms_scaled(latent, latent_gain).astype(jnp.bfloat16)
-    packed = key_turned.reshape(2, 16, 16, ROPE).transpose(0, 2, 1, 3).reshape(2, KT_ROWS, 512)
-    own = jnp.concatenate([packed, normed.reshape(2, HALF_ROWS, 512)], axis=1)
-    wup = jnp.concatenate([key_up_second, key_up_first, value_up_first, value_up_second], axis=1)
-    return attend(own, q1, q2, wup, out_first, out_second, residual, expert_gain.reshape(1, -1))
-
-
-def clamped_unit(gate, upward):
-    limited = jnp.minimum(gate, 7.0)
-    bounded = jnp.clip(upward, -7.0, 7.0)
-    return (bounded + 1.0) * limited * jax.nn.sigmoid(1.702 * limited)
-
-
-def slot_numbers(chosen, experts):
-    hits = (chosen[..., None] == jnp.arange(experts, dtype=jnp.int32)).astype(jnp.int32)
-    before = jnp.cumsum(hits, axis=-2) - hits
-    return chosen * CAP + jnp.sum(before * hits, axis=-1)
-
-
-def expert_hidden(rows, gate_weight, up_weight):
-    gate = jnp.einsum("nsecd,edf->nsecf", rows, gate_weight, preferred_element_type=jnp.float32)
-    upward = jnp.einsum("nsecd,edf->nsecf", rows, up_weight, preferred_element_type=jnp.float32)
-    return clamped_unit(gate, upward).astype(jnp.bfloat16)
+    me = lax.axis_index("sp")
+    tp = lax.axis_index("tp")
+    core = lax.rem(tp, 2)
+    z = lax.div(tp, 2)
+    zn = lax.axis_size("tp") // 2
+    far = zn // 2
+    sib = {"sp": me, "tp": tp + 1 - 2 * core}
+    z_up = {"sp": me, "tp": lax.rem(z + 1, zn) * 2 + core}
+    z_dn = {"sp": me, "tp": lax.rem(z + zn - 1, zn) * 2 + core}
+    peers = [sib, z_up, z_dn]
+
+    loads = [
+        pltpu.make_async_copy(gate_hbm, wgu.at[:, :, pl.ds(0, 256)], w_sem.at[0]),
+        pltpu.make_async_copy(up_hbm, wgu.at[:, :, pl.ds(256, 256)], w_sem.at[1]),
+        pltpu.make_async_copy(down_hbm, wdn, w_sem.at[2]),
+        pltpu.make_async_copy(own, gx.at[z, core], w_sem.at[3]),
+    ]
+    for load in loads:
+        load.start()
+    barrier = pltpu.get_barrier_semaphore()
+    for peer in peers:
+        pl.semaphore_signal(barrier, inc=1, device_id=peer, device_id_type=MESH_ID)
+    pl.semaphore_wait(barrier, len(peers))
+
+    def at(shift):
+        return lax.rem(z + shift + zn, zn)
+
+    def g_copy(direction, hop, e):
+        chip = at(-hop if direction == 0 else hop)
+        return pltpu.make_async_remote_copy(
+            src_ref=own.at[e] if hop == 0 else gx.at[chip, core, e],
+            dst_ref=gx.at[chip, core, e],
+            send_sem=g_send.at[direction, hop, e], recv_sem=g_recv.at[direction, hop, e],
+            device_id=z_up if direction == 0 else z_dn, device_id_type=MESH_ID,
+        )
+
+    def g_wait(direction, hop, e):
+        chip = at(-hop if direction == 0 else hop)
+        pltpu.make_async_remote_copy(
+            src_ref=gx.at[chip, core, e], dst_ref=gx.at[chip, core, e],
+            send_sem=g_send.at[direction, hop - 1, e], recv_sem=g_recv.at[direction, hop - 1, e],
+            device_id=z_up, device_id_type=MESH_ID,
+        ).wait_recv()
+
+    def s_copy(shift, e, mine):
+        chip = at(shift)
+        half = core if mine else 1 - core
+        slot = (shift + zn) % zn
+        return pltpu.make_async_remote_copy(
+            src_ref=own.at[e] if shift == 0 and mine else gx.at[chip, half, e], dst_ref=gx.at[chip, half, e],
+            send_sem=s_send.at[slot, e], recv_sem=s_recv.at[slot, e],
+            device_id=sib, device_id_type=MESH_ID,
+        )
+
+    def x_copy(shift, e):
+        chip = at(shift)
+        slot = (shift + zn) % zn
+        return pltpu.make_async_remote_copy(
+            src_ref=py.at[1 - core, chip, e], dst_ref=pd.at[chip, e],
+            send_sem=x_send.at[slot, e], recv_sem=x_recv.at[slot, e],
+            device_id=sib, device_id_type=MESH_ID,
+        )
+
+    for e in (0, 1):
+        for direction in (0, 1):
+            g_copy(direction, 0, e).start()
+    for e in (0, 1):
+        s_copy(0, e, True).start()
+
+    def compute(shifts):
+        chips = [at(shift) for shift in shifts]
+
+        def one(e, _):
+            rows = jnp.concatenate([gx[chip, half, e] for chip in chips for half in (0, 1)], axis=0)
+            hidden = jnp.dot(rows, wgu[e], preferred_element_type=jnp.float32)
+            gate = jnp.minimum(hidden[:, :256], 7.0)
+            up = jnp.clip(hidden[:, 256:], -7.0, 7.0)
+            act = ((up + 1.0) * gate * (1.0 / (1.0 + jnp.exp(-1.702 * gate)))).astype(jnp.bfloat16)
+            part = jnp.dot(act, wdn[e], preferred_element_type=jnp.float32).astype(jnp.bfloat16)
+            for number, chip in enumerate(chips):
+                for half in (0, 1):
+                    py[half, chip, e] = part[(2 * number + half) * 48:(2 * number + half) * 48 + 48]
+            return 0
+
+        lax.fori_loop(0, 2, one, 0)
+        for shift in shifts:
+            for e in (0, 1):
+                x_copy(shift, e).start()
+
+    for load in loads:
+        load.wait()
+    for e in (0, 1):
+        s_copy(0, e, False).wait_recv()
+    compute([0])
+
+    for hop in range(1, far + 1):
+        for e in (0, 1):
+            for direction in (0, 1):
+                if hop == far and e != direction:
+                    continue
+                g_wait(direction, hop, e)
+                if hop < far - 1 or (hop == far - 1 and e == direction):
+                    g_copy(direction, hop, e).start()
+                s_copy(-hop if direction == 0 else hop, e, True).start()
+        shifts = [-hop, hop] if hop < far else [far]
+        for shift in shifts:
+            for e in (0, 1):
+                s_copy(shift, e, False).wait_recv()
+        compute(shifts)
+
+    def pair_sum(shift, e):
+        chip = at(shift)
+        return py[core, chip, e].astype(jnp.float32) + pd[chip, e].astype(jnp.float32)
+
+    def r_copy(direction, hop, e):
+        return pltpu.make_async_remote_copy(
+            src_ref=rs_out.at[direction, hop, e], dst_ref=rs_in.at[direction, hop, e],
+            send_sem=r_send.at[direction, hop, e], recv_sem=r_recv.at[direction, hop, e],
+            device_id=z_up if direction == 0 else z_dn, device_id_type=MESH_ID,
+        )
+
+    seen = set()
+    used = []
+    for hop, flip in ((0, 0), (1, 1), (1, 0), (2, 1), (2, 0), (3, 1), (3, 0)):
+        for direction in (0, 1):
+            e = direction if flip == 0 else 1 - direction
+            shift = (far - hop) if direction == 0 else -(far - hop)
+            key = (shift % zn, e)
+            if key not in seen:
+                seen.add(key)
+                x_copy(shift, e).wait_recv()
+            total = pair_sum(shift, e)
+            if hop > 0 and not (hop == 1 and e != direction):
+                r_copy(direction, hop - 1, e).wait_recv()
+                total = total + rs_in[direction, hop - 1, e].astype(jnp.float32)
+            rs_out[direction, hop, e] = total.astype(jnp.bfloat16)
+            r_copy(direction, hop, e).start()
+            used.append((direction, hop, e))
+    for e in (0, 1):
+        x_copy(0, e).wait_recv()
+        total = pair_sum(0, e)
+        for direction in (0, 1):
+            r_copy(direction, far - 1, e).wait_recv()
+            total = total + rs_in[direction, far - 1, e].astype(jnp.float32)
+        out_ref[e] = total.astype(jnp.bfloat16)
+
+    for item in used:
+        r_copy(*item).wait_send()
+    for e in (0, 1):
+        for shift in range(-far + 1, far + 1):
+            s_copy(shift, e, True).wait_send()
+            x_copy(shift, e).wait_send()
+        for direction in (0, 1):
+            for hop in range(far):
+                if hop < far - 1 or e == direction:
+                    g_copy(direction, hop, e).wait_send()
+
+
+def run_experts(rows, gate_weight, up_weight, down_weight):
+    vmem = pl.BlockSpec(memory_space=pltpu.VMEM)
+    hbm = pl.BlockSpec(memory_space=pl.ANY)
+    bf16 = jnp.bfloat16
+    dma = pltpu.SemaphoreType.DMA
+    return pl.pallas_call(
+        expert_kernel,
+        out_shape=jax.ShapeDtypeStruct((2, 48, 2048), bf16),
+        in_specs=[vmem, hbm, hbm, hbm],
+        out_specs=vmem,
+        scratch_shapes=[
+            pltpu.VMEM((8, 2, 2, 48, 2048), bf16),
+            pltpu.VMEM((2, 8, 2, 48, 2048), bf16),
+            pltpu.VMEM((8, 2, 48, 2048), bf16),
+            pltpu.VMEM((2, 2048, 512), bf16),
+            pltpu.VMEM((2, 256, 2048), bf16),
+            pltpu.VMEM((2, 4, 2, 48, 2048), bf16),
+            pltpu.VMEM((2, 4, 2, 48, 2048), bf16),
+            dma((4,)), dma((2, 4, 2)), dma((2, 4, 2)), dma((8, 2)), dma((8, 2)),
+            dma((8, 2)), dma((8, 2)), dma((2, 4, 2)), dma((2, 4, 2)),
+        ],
+        compiler_params=pltpu.CompilerParams(collective_id=2, has_side_effects=True, vmem_limit_bytes=56 * 2**20),
+        name="experts",
+    )(rows, gate_weight, up_weight, down_weight)
 
 
 def body(
@@ -381,38 +606,21 @@
     key_up_second, value_up_second, out_first, out_second, residual, expert_gain,
     route_experts, route_scores, gate_weight, up_weight, down_weight,
 ):
-    middle, normed = attention_part(
-        query_first, query_second, latent, key_rotary, latent_gain, key_up_first, value_up_first,
-        key_up_second, value_up_second, out_first, out_second, residual, expert_gain,
+    middle, outgoing, mix = attend(
+        query_first.T, query_second.T, latent, key_rotary.T, latent_gain.reshape(1, -1), key_up_first.T, value_up_first.T,
+        key_up_second, value_up_second, out_first, out_second, residual, expert_gain.reshape(1, -1),
+        route_experts.T, route_scores.T,
     )
-    sets = lax.axis_size("tp")
     groups = lax.axis_size("sp")
-    own_rows = latent.shape[0] // sets
-    topk = route_experts.shape[1]
     local_experts = gate_weight.shape[0]
-    experts = local_experts * groups
-    own_start = lax.axis_index("tp") * own_rows
-    slot_range = jnp.arange(experts * CAP, dtype=jnp.int32)
-    own_ids = lax.dynamic_slice_in_dim(route_experts, own_start, own_rows, 0).reshape(-1)
-    own_slots = slot_numbers(own_ids, experts)
-    picks = (own_slots[:, None] == slot_range).reshape(own_rows, topk, experts * CAP)
-    selected = jnp.sum(picks.astype(jnp.float32), axis=1).astype(jnp.bfloat16)
-    outgoing = jnp.einsum("ts,td->sd", selected, normed, preferred_element_type=jnp.float32).astype(jnp.bfloat16)
     outgoing = outgoing.reshape(groups, local_experts, CAP, outgoing.shape[-1])
     arrived = lax.all_to_all(outgoing, "sp", split_axis=0, concat_axis=0, tiled=True)
-    activated = expert_hidden(lax.all_gather(arrived[None], "tp", axis=0, tiled=True), gate_weight, up_weight)
-    flat_hidden = activated.reshape(sets * groups, local_experts, CAP, activated.shape[-1])
-    summed = lax.psum_scatter(
-        jnp.einsum("secf,efd->secd", flat_hidden, down_weight, preferred_element_type=jnp.float32).astype(jnp.bfloat16),
-        "tp", scatter_dimension=0, tiled=True,
-    )
+    rows = arrived.transpose(1, 0, 2, 3).reshape(local_experts, groups * CAP, -1)
+    summed = run_experts(rows, gate_weight, up_weight, down_weight)
+    summed = summed.reshape(local_experts, groups, CAP, -1).transpose(1, 0, 2, 3)
     returned = lax.all_to_all(summed, "sp", split_axis=0, concat_axis=0, tiled=True)
-    expert_out = returned.reshape(experts * CAP, returned.shape[-1]).astype(jnp.float32)
-    own_scores = lax.dynamic_slice_in_dim(route_scores, own_start, own_rows, 0)
-    route_weight = jax.nn.softmax(own_scores, axis=-1)
-    matches = own_slots.reshape(own_rows, topk)[..., None] == slot_range
-    combine = jnp.sum(jnp.where(matches, route_weight[..., None], 0.0), axis=1)
-    mixture = jnp.dot(combine, expert_out)
+    expert_out = returned.reshape(groups * local_experts * CAP, returned.shape[-1]).astype(jnp.float32)
+    mixture = jnp.dot(mix, expert_out)
     return (middle.astype(jnp.float32) + mixture).astype(jnp.bfloat16)
 
 

time: 262 us -> 172 us (0.66)
  waiting for transfers between devices: 108 us -> 0 us
  Pallas kernels: 62.8 us -> 133 us
  local copies, waits for them, and re-layouts: 24.3 us -> 4.85 us
  between operations: 13.7 us -> 0.08 us
  matrix products: 9.56 us -> 0.85 us
  other arithmetic: 8.61 us -> 0 us
    pallas_call x0 -> x1, Pallas kernels: none -> 73.8 us  [run_experts(): pl.pallas_call(expert_kernel, out_shape=jax.ShapeDtypeStruct((2, 48, 2048...]
    reduce_scatter x1 -> x0, waiting for transfers between devices: 65.9 us -> none  [body(): lax.psum_scatter(jnp.einsum('secf,efd->secd', flat_hidden, down_weight, p...]
    all_gather x1 -> x0, waiting for transfers between devices: 42.1 us -> none  [body(): lax.all_gather(arrived[None], 'tp', axis=0, tiled=True)]
    dot_general x5 -> x1, matrix products: 9.56 us -> 0.85 us  [body(): mixture = jnp.dot(mix, expert_out)]
    unnamed x36 -> x4, local copies, waits for them, and re-layouts: 7.69 us -> 0.01 us
    all_gather x1 -> x0, local copies, waits for them, and re-layouts: 5.83 us -> none  [body(): lax.all_gather(arrived[None], 'tp', axis=0, tiled=True)]
    slice x4 -> x0, local copies, waits for them, and re-layouts: 4.08 us -> none  [the longest x2 2.41 us: turned(): pieces = [query[:, :nope]]]
    pallas_call x1, Pallas kernels: 62.8 us -> 59.6 us  [attend(): pl.pallas_call(attend_kernel, out_shape=[jax.ShapeDtypeStruct((32, 2048),...]
  transfers between devices with their start and end apart: 2 -> 0, of which waited for: 2 -> 0; matrix products, arithmetic and copies ran while one was open for 0% -> 0% of each run, Pallas kernels for 0% -> 0%
where the time goes in v2:
time: 172 us
  Pallas kernels  133 us (77%)
  blocking collectives  33.1 us (19%)
  local copies, waits for them, and re-layouts  4.85 us (3%)
    pallas_call x1, Pallas kernels, run_experts(): pl.pallas_call(expert_kernel, out_shape=jax.ShapeDtypeStruct((2, 48, 2048...  73.8 us
    pallas_call x1, Pallas kernels, attend(): pl.pallas_call(attend_kernel, out_shape=[jax.ShapeDtypeStruct((32, 2048),...  59.6 us
    all_to_all x1, blocking collectives, body(): lax.all_to_all(outgoing, 'sp', split_axis=0, concat_axis=0, tiled=True)  20.8 us
    all_to_all x1, blocking collectives, body(): lax.all_to_all(summed, 'sp', split_axis=0, concat_axis=0, tiled=True)  12.3 us

profile of v2, /device:TPU:2, one launch (start us, length us, event | category | flops | bytes accessed | tf_op | source)
XLA Modules:
  0.0 172.2 jit_solution(7651259594260235442)
XLA Ops:
  0.0 59.6 %gather_attend.1 = (bf16[32,2048]{1,0:T(8,128)(2,1)}, bf16[96,2048]{1,0:T(8,128)(2,1)}, f32[32,96]{1,0:T(8,128)}) custom-call(bf16[96,512]{1,0:T(8,128)(2,1)} %bitcast.20, bf16[160,512]{1,0:T(8,128)(2,1)} %bitcast.19, bf16[512,512]{1,0:T(8,128)(2,1)} %lat_hbm.1, bf16[32,512]{1,0:T(8,128)(2,1)} %bitcast.23, f32[1,512]{1,0:T(1,128)} %bitcast.27, ...), custom_call_target="tpu_custom_call" | custom-call | tf_op jit(solution)/shard_map/gather_attend/pallas_call | solution.py:380
  59.6 1.4 reshape.20
  61.0 0.5 copy.26
  61.5 20.8 %all_to_all.10 = bf16[16,2,3,2048]{3,1,2,0:T(2,128)(2,1)S(1)} all-to-all(bf16[16,2,3,2048]{3,1,2,0:T(2,128)(2,1)S(1)} %copy.26), channel_id=1, replica_groups=mesh['sp'=16,'tp'=16] {'sp'}, dimensions={0} | all-to-all | bytes 786432 | tf_op jit(solution)/shard_map/all_to_all | solution.py:617
  82.3 0.9 copy.27.own
  83.2 73.8 %experts.1 = bf16[2,48,2048]{2,1,0:T(8,128)(2,1)} custom-call(bf16[2,48,2048]{2,1,0:T(8,128)(2,1)} %copy.27.own, bf16[2,2048,256]{2,1,0:T(8,128)(2,1)} %gate_hbm.1, bf16[2,2048,256]{2,1,0:T(8,128)(2,1)} %up_hbm.1, bf16[2,256,2048]{2,1,0:T(8,128)(2,1)} %down_hbm.1), custom_call_target="tpu_custom_call" | custom-call | tf_op jit(solution)/shard_map/experts/pallas_call | solution.py:583
  156.9 0.0 copy-start
  156.9 0.0 copy-start.1
  157.0 1.4 copy.28
  158.4 12.3 %all_to_all.11 = bf16[16,2,3,2048]{3,1,2,0:T(2,128)(2,1)S(1)} all-to-all(bf16[16,2,3,2048]{3,1,2,0:T(2,128)(2,1)S(1)} %bitcast.18), channel_id=1, replica_groups=mesh['sp'=16,'tp'=16] {'sp'}, dimensions={0} | all-to-all | bytes 786432 | tf_op jit(solution)/shard_map/all_to_all | solution.py:621
  170.7 0.3 copy.29
  171.0 0.3 reshape.23
  171.3 0.0 copy-done
  171.3 0.0 copy-done.1
  171.3 0.8 fusion
Async XLA Ops:
  156.9 14.4 %copy-start = (bf16[32,2048]{1,0:T(8,128)(2,1)S(1)}, bf16[32,2048]{1,0:T(8,128)(2,1)}, u32[]{:S(2)}) copy-start(bf16[32,2048]{1,0:T(8,128)(2,1)} %get-tuple-element.8) | copy-start | bytes 393220
  156.9 14.4 %copy-start.1 = (f32[32,96]{1,0:T(8,128)S(1)}, f32[32,96]{1,0:T(8,128)}, u32[]{:S(2)}) copy-start(f32[32,96]{1,0:T(8,128)} %get-tuple-element.9) | copy-start | bytes 36868

commit v3 on v2

--- a/solution.py
+++ b/solution.py
@@ -14,6 +14,7 @@
 HALF_ROWS = 256
 KT_ROWS = 16
 PIECE = HALF_ROWS + KT_ROWS
+A_SCRATCH = 42
 CUT = 144
 MESH_ID = pl.DeviceIdType.MESH
 STEPS = (
@@ -31,7 +32,7 @@
 
 
 def attend_kernel(
-    qf_hbm, qs_hbm, lat_hbm, kr_hbm, latg_hbm, kuf_hbm, vuf_hbm, kus_hbm, vus_hbm,
+    weight_loads, qf_hbm, qs_hbm, lat_hbm, kr_hbm, latg_hbm, kuf_hbm, vuf_hbm, kus_hbm, vus_hbm,
     of_hbm, os_hbm, res_hbm, gain_hbm, ids_hbm, scores_hbm, base_hbm, start_hbm,
     mid_ref, out_ref, mix_ref,
     qf, qs, lat, kr, latg, kuf, vuf, kus, vus, gain, ids, scores, base, start,
@@ -58,7 +59,8 @@
     sib = {"sp": me, "tp": tp + 1 - 2 * core}
     z_up = {"sp": me, "tp": lax.rem(z + 1, zn) * 2 + core}
     z_dn = {"sp": me, "tp": lax.rem(z + zn - 1, zn) * 2 + core}
-    peers = [sp_dev(1, 0), sp_dev(-1, 0), sp_dev(0, 1), sp_dev(0, -1), sib, z_up, z_dn]
+    groups = lax.axis_size("sp")
+    peers = [sib, z_up, z_dn] + [{"sp": lax.rem(me + k, groups), "tp": tp} for k in range(1, groups)]
 
     mine = pl.ds(pl.multiple_of(tp * 32, 32), 32)
     pairs = [
@@ -68,7 +70,7 @@
         (gain_hbm, gain), (ids_hbm, ids), (scores_hbm, scores),
     ]
     loads = [pltpu.make_async_copy(a, b, loc_sem.at[n]) for n, (a, b) in enumerate(pairs)]
-    for load in loads:
+    for load in loads + weight_loads:
         load.start()
     wout[pl.ds(0, 64)] = jnp.zeros((64, wout.shape[1]), wout.dtype)
     m1[...] = jnp.full(m1.shape, MASKED, jnp.float32)
@@ -338,7 +340,7 @@
     mid_ref[...] = mid
     wide = mid.astype(jnp.float32)
     normed = (wide * lax.rsqrt(jnp.mean(wide * wide, axis=1, keepdims=True) + EPS) * gain[...]).astype(bf16)
-    slots = out_ref.shape[0]
+    slots = mix_ref.shape[1]
     token = lax.broadcasted_iota(jnp.int32, (32, 512), 1) == lax.broadcasted_iota(jnp.int32, (32, 512), 0) + tp * 32
     names = [jnp.sum(jnp.where(token, ids[k:k + 1], 0), axis=1, keepdims=True) for k in (0, 1)]
     logits = [jnp.sum(jnp.where(token, scores[k:k + 1], 0.0), axis=1, keepdims=True) for k in (0, 1)]
@@ -350,21 +352,244 @@
     picked, mix = 0.0, 0.0
     for k in (0, 1):
         rank = jnp.sum(before * hits[k], axis=1, keepdims=True)
-        slot = names[k] * CAP + rank.astype(jnp.int32)
+        slot = (names[k] >> 1) * 8 + (names[k] & 1) * CAP + rank.astype(jnp.int32)
         here = (lax.broadcasted_iota(jnp.int32, (32, slots), 1) == slot).astype(f32)
         picked = picked + here
         mix = mix + here * (powers[k] / (powers[0] + powers[1]))
     mix_ref[...] = mix
     out_ref[...] = lax.dot_general(
         picked.astype(bf16), normed, (((0,), (0,)), ((), ())), preferred_element_type=f32
-    ).astype(bf16)
+    ).astype(bf16).reshape(out_ref.shape)
     for d in order:
         x_copy(d).wait_send()
     for item in used:
         r_copy(*item).wait_send()
 
 
-def attend(*args):
+def expert_kernel(
+    going, mid, mix, loads, out_ref,
+    a_in, b_out, b_in, own, gx, py, pd, wgu, wdn, rs_out, rs_in,
+    a_send, a_recv, b_send, b_recv, g_send, g_recv, s_send, s_recv, x_send, x_recv, r_send, r_recv,
+):
+    me = lax.axis_index("sp")
+    tp = lax.axis_index("tp")
+    core = lax.rem(tp, 2)
+    z = lax.div(tp, 2)
+    zn = lax.axis_size("tp") // 2
+    far = zn // 2
+    sib = {"sp": me, "tp": tp + 1 - 2 * core}
+    z_up = {"sp": me, "tp": lax.rem(z + 1, zn) * 2 + core}
+    z_dn = {"sp": me, "tp": lax.rem(z + zn - 1, zn) * 2 + core}
+    groups = lax.axis_size("sp")
+
+    def exchange(k, src, dst, send_sems, recv_sems):
+        peer = lax.rem(me + k, groups)
+        return pltpu.make_async_remote_copy(
+            src_ref=src.at[peer, pl.ds(0, 6)], dst_ref=dst.at[me, pl.ds(0, 6)], send_sem=send_sems.at[k], recv_sem=recv_sems.at[k],
+            device_id={"sp": peer, "tp": tp}, device_id_type=MESH_ID,
+        )
+
+    def exchanged(k, dst, send_sems, recv_sems):
+        peer = lax.rem(me + groups - k, groups)
+        pltpu.make_async_remote_copy(
+            src_ref=dst.at[peer, pl.ds(0, 6)], dst_ref=dst.at[peer, pl.ds(0, 6)], send_sem=send_sems.at[k], recv_sem=recv_sems.at[k],
+            device_id={"sp": peer, "tp": tp}, device_id_type=MESH_ID,
+        ).wait_recv()
+
+    def each(act):
+        def one(k, _):
+            act(k)
+            return 0
+
+        lax.fori_loop(1, groups, one, 0)
+
+    each(lambda k: exchange(k, going, a_in, a_send, a_recv).start())
+    a_in[me] = going[me]
+    row = lax.broadcasted_iota(jnp.int32, (96, 128), 0)
+    col = lax.broadcasted_iota(jnp.int32, (96, 128), 1)
+    inner = col & 7
+    second = (inner >= CAP).astype(jnp.int32)
+    wanted = second * 48 + (col >> 3) * CAP + inner - second * CAP
+    compact = ((row == wanted) & (inner < 2 * CAP)).astype(jnp.float32).astype(jnp.bfloat16)
+    each(lambda k: exchanged(k, a_in, a_send, a_recv))
+    own[...] = jnp.dot(
+        compact, a_in[...].reshape(128, 2048), preferred_element_type=jnp.float32
+    ).astype(jnp.bfloat16).reshape(own.shape)
+    gx[z, core] = own[...]
+    each(lambda k: exchange(k, going, a_in, a_send, a_recv).wait_send())
+
+    def at(shift):
+        return lax.rem(z + shift + zn, zn)
+
+    def g_copy(direction, hop, e):
+        chip = at(-hop if direction == 0 else hop)
+        return pltpu.make_async_remote_copy(
+            src_ref=own.at[e] if hop == 0 else gx.at[chip, core, e],
+            dst_ref=gx.at[chip, core, e],
+            send_sem=g_send.at[direction, hop, e], recv_sem=g_recv.at[direction, hop, e],
+            device_id=z_up if direction == 0 else z_dn, device_id_type=MESH_ID,
+        )
+
+    def g_wait(direction, hop, e):
+        chip = at(-hop if direction == 0 else hop)
+        pltpu.make_async_remote_copy(
+            src_ref=gx.at[chip, core, e], dst_ref=gx.at[chip, core, e],
+            send_sem=g_send.at[direction, hop - 1, e], recv_sem=g_recv.at[direction, hop - 1, e],
+            device_id=z_up, device_id_type=MESH_ID,
+        ).wait_recv()
+
+    def s_copy(shift, e, mine):
+        chip = at(shift)
+        half = core if mine else 1 - core
+        slot = (shift + zn) % zn
+        return pltpu.make_async_remote_copy(
+            src_ref=own.at[e] if shift == 0 and mine else gx.at[chip, half, e], dst_ref=gx.at[chip, half, e],
+            send_sem=s_send.at[slot, e], recv_sem=s_recv.at[slot, e],
+            device_id=sib, device_id_type=MESH_ID,
+        )
+
+    def x_copy(shift, e):
+        chip = at(shift)
+        slot = (shift + zn) % zn
+        return pltpu.make_async_remote_copy(
+            src_ref=py.at[1 - core, chip, e], dst_ref=pd.at[chip, e],
+            send_sem=x_send.at[slot, e], recv_sem=x_recv.at[slot, e],
+            device_id=sib, device_id_type=MESH_ID,
+        )
+
+    for e in (0, 1):
+        for direction in (0, 1):
+            g_copy(direction, 0, e).start()
+    for e in (0, 1):
+        s_copy(0, e, True).start()
+
+    def compute(shifts):
+        chips = [at(shift) for shift in shifts]
+
+        def one(e, _):
+            rows = jnp.concatenate([gx[chip, half, e] for chip in chips for half in (0, 1)], axis=0)
+            hidden = jnp.dot(rows, wgu[e], preferred_element_type=jnp.float32)
+            gate = jnp.minimum(hidden[:, :256], 7.0)
+            up = jnp.clip(hidden[:, 256:], -7.0, 7.0)
+            act = ((up + 1.0) * gate * (1.0 / (1.0 + jnp.exp(-1.702 * gate)))).astype(jnp.bfloat16)
+            part = jnp.dot(act, wdn[e], preferred_element_type=jnp.float32).astype(jnp.bfloat16)
+            for number, chip in enumerate(chips):
+                for half in (0, 1):
+                    py[half, chip, e] = part[(2 * number + half) * 48:(2 * number + half) * 48 + 48]
+            return 0
+
+        lax.fori_loop(0, 2, one, 0)
+        for shift in shifts:
+            for e in (0, 1):
+                x_copy(shift, e).start()
+
+    for load in loads:
+        load.wait()
+    for e in (0, 1):
+        s_copy(0, e, False).wait_recv()
+    compute([0])
+
+    def pair_sum(shift, e):
+        chip = at(shift)
+        return py[core, chip, e].astype(jnp.float32) + pd[chip, e].astype(jnp.float32)
+
+    def r_copy(direction, hop, e):
+        return pltpu.make_async_remote_copy(
+            src_ref=rs_out.at[direction, hop, e], dst_ref=rs_in.at[direction, hop, e],
+            send_sem=r_send.at[direction, hop, e], recv_sem=r_recv.at[direction, hop, e],
+            device_id=z_up if direction == 0 else z_dn, device_id_type=MESH_ID,
+        )
+
+    seen = set()
+    used = []
+
+    def ring(hop, flip):
+        for direction in (0, 1):
+            e = direction if flip == 0 else 1 - direction
+            shift = (far - hop) if direction == 0 else -(far - hop)
+            key = (shift % zn, e)
+            if key not in seen:
+                seen.add(key)
+                x_copy(shift, e).wait_recv()
+            total = pair_sum(shift, e)
+            if hop > 0 and not (hop == 1 and e != direction):
+                r_copy(direction, hop - 1, e).wait_recv()
+                total = total + rs_in[direction, hop - 1, e].astype(jnp.float32)
+            rs_out[direction, hop, e] = total.astype(jnp.bfloat16)
+            r_copy(direction, hop, e).start()
+            used.append((direction, hop, e))
+
+    for hop in range(1, far + 1):
+        if hop == far:
+            ring(1, 1)
+        for e in (0, 1):
+            for direction in (0, 1):
+                if hop == far and e != direction:
+                    continue
+                g_wait(direction, hop, e)
+                if hop < far - 1 or (hop == far - 1 and e == direction):
+                    g_copy(direction, hop, e).start()
+                s_copy(-hop if direction == 0 else hop, e, True).start()
+        shifts = [-hop, hop] if hop < far else [far]
+        for shift in shifts:
+            for e in (0, 1):
+                s_copy(shift, e, False).wait_recv()
+        compute(shifts)
+
+    for item in ((0, 0), (2, 1), (1, 0), (3, 1), (2, 0), (3, 0)):
+        ring(*item)
+    sums = []
+    for e in (0, 1):
+        x_copy(0, e).wait_recv()
+        total = pair_sum(0, e)
+        for direction in (0, 1):
+            r_copy(direction, far - 1, e).wait_recv()
+            total = total + rs_in[direction, far - 1, e].astype(jnp.float32)
+        sums.append(total.astype(jnp.bfloat16))
+    b_out[...] = lax.dot_general(
+        compact, jnp.concatenate(sums, axis=0), (((0,), (0,)), ((), ())), preferred_element_type=jnp.float32
+    ).astype(jnp.bfloat16).reshape(b_out.shape)
+    each(lambda k: exchange(k, b_out, b_in, b_send, b_recv).start())
+    b_in[me] = b_out[me]
+    each(lambda k: exchanged(k, b_in, b_send, b_recv))
+    mixture = jnp.dot(
+        mix[...], b_in[...].reshape(128, 2048).astype(jnp.float32),
+        preferred_element_type=jnp.float32, precision=lax.Precision.HIGHEST,
+    )
+    out_ref[...] = (mid[...].astype(jnp.float32) + mixture).astype(jnp.bfloat16)
+    each(lambda k: exchange(k, b_out, b_in, b_send, b_recv).wait_send())
+
+    for item in used:
+        r_copy(*item).wait_send()
+    for e in (0, 1):
+        for shift in range(-far + 1, far + 1):
+            s_copy(shift, e, True).wait_send()
+            x_copy(shift, e).wait_send()
+        for direction in (0, 1):
+            for hop in range(far):
+                if hop < far - 1 or e == direction:
+                    g_copy(direction, hop, e).wait_send()
+
+
+def layer_kernel(*refs):
+    ins, weights, out_ref = refs[:17], refs[17:20], refs[20]
+    middles, first = refs[21:24], refs[24:24 + A_SCRATCH]
+    rest = refs[24 + A_SCRATCH:]
+    w_sem, second = rest[0], rest[1:]
+    a_in, b_in, wgu, wdn = second[0], second[2], second[7], second[8]
+    loads = [
+        pltpu.make_async_copy(weights[0], wgu.at[:, :, pl.ds(0, 256)], w_sem.at[0]),
+        pltpu.make_async_copy(weights[1], wgu.at[:, :, pl.ds(256, 256)], w_sem.at[1]),
+        pltpu.make_async_copy(weights[2], wdn, w_sem.at[2]),
+    ]
+    for ref in (a_in, b_in):
+        ref[...] = jnp.zeros(ref.shape, ref.dtype)
+    attend_kernel(loads, *ins, *middles, *first)
+    mid, going, mix = middles
+    expert_kernel(going, mid, mix, loads, out_ref, *second)
+
+
+def layer(*args):
     hbm = pl.BlockSpec(memory_space=pltpu.HBM)
     vmem = pl.BlockSpec(memory_space=pltpu.VMEM)
     f32, bf16 = jnp.float32, jnp.bfloat16
@@ -377,15 +602,7 @@
     live = lanes < ROPE
     base = np.stack([np.cos(place * speed) * live, np.sin(place * speed) * live]).astype(np.float32)
     start = np.stack([np.cos(first * speed) * live, np.sin(first * speed) * live]).astype(np.float32)
-    return pl.pallas_call(
-        attend_kernel,
-        out_shape=[
-            jax.ShapeDtypeStruct((32, 2048), bf16), jax.ShapeDtypeStruct((96, 2048), bf16),
-            jax.ShapeDtypeStruct((32, 96), f32),
-        ],
-        in_specs=[hbm] * 17,
-        out_specs=[vmem] * 3,
-        scratch_shapes=[
+    scratch_a = [
             pltpu.VMEM((96, 512), bf16), pltpu.VMEM((160, 512), bf16), pltpu.VMEM((512, 512), bf16),
             pltpu.VMEM((32, 512), bf16), pltpu.VMEM((1, 512), f32),
             pltpu.VMEM((64, 512), bf16), pltpu.VMEM((64, 512), bf16),
@@ -406,186 +623,10 @@
             pltpu.VMEM((2, 4, 2, 32, 1024), bf16),
             dma((20,)), dma((20,)), dma((15,)), dma((15,)), dma((17,)),
             dma((8,)), dma((8,)), dma((2, 4, 2)), dma((2, 4, 2)),
-        ],
-        compiler_params=pltpu.CompilerParams(collective_id=1, has_side_effects=True, vmem_limit_bytes=67043328),
-        name="gather_attend",
-    )(*args, jnp.asarray(base), jnp.asarray(start))
-
-
-def expert_kernel(
-    own, gate_hbm, up_hbm, down_hbm, out_ref,
-    gx, py, pd, wgu, wdn, rs_out, rs_in,
-    w_sem, g_send, g_recv, s_send, s_recv, x_send, x_recv, r_send, r_recv,
-):
-    me = lax.axis_index("sp")
-    tp = lax.axis_index("tp")
-    core = lax.rem(tp, 2)
-    z = lax.div(tp, 2)
-    zn = lax.axis_size("tp") // 2
-    far = zn // 2
-    sib = {"sp": me, "tp": tp + 1 - 2 * core}
-    z_up = {"sp": me, "tp": lax.rem(z + 1, zn) * 2 + core}
-    z_dn = {"sp": me, "tp": lax.rem(z + zn - 1, zn) * 2 + core}
-    peers = [sib, z_up, z_dn]
-
-    loads = [
-        pltpu.make_async_copy(gate_hbm, wgu.at[:, :, pl.ds(0, 256)], w_sem.at[0]),
-        pltpu.make_async_copy(up_hbm, wgu.at[:, :, pl.ds(256, 256)], w_sem.at[1]),
-        pltpu.make_async_copy(down_hbm, wdn, w_sem.at[2]),
-        pltpu.make_async_copy(own, gx.at[z, core], w_sem.at[3]),
-    ]
-    for load in loads:
-        load.start()
-    barrier = pltpu.get_barrier_semaphore()
-    for peer in peers:
-        pl.semaphore_signal(barrier, inc=1, device_id=peer, device_id_type=MESH_ID)
-    pl.semaphore_wait(barrier, len(peers))
-
-    def at(shift):
-        return lax.rem(z + shift + zn, zn)
-
-    def g_copy(direction, hop, e):
-        chip = at(-hop if direction == 0 else hop)
-        return pltpu.make_async_remote_copy(
-            src_ref=own.at[e] if hop == 0 else gx.at[chip, core, e],
-            dst_ref=gx.at[chip, core, e],
-            send_sem=g_send.at[direction, hop, e], recv_sem=g_recv.at[direction, hop, e],
-            device_id=z_up if direction == 0 else z_dn, device_id_type=MESH_ID,
-        )
-
-    def g_wait(direction, hop, e):
-        chip = at(-hop if direction == 0 else hop)
-        pltpu.make_async_remote_copy(
-            src_ref=gx.at[chip, core, e], dst_ref=gx.at[chip, core, e],
-            send_sem=g_send.at[direction, hop - 1, e], recv_sem=g_recv.at[direction, hop - 1, e],
-            device_id=z_up, device_id_type=MESH_ID,
-        ).wait_recv()
-
-    def s_copy(shift, e, mine):
-        chip = at(shift)
-        half = core if mine else 1 - core
-        slot = (shift + zn) % zn
-        return pltpu.make_async_remote_copy(
-            src_ref=own.at[e] if shift == 0 and mine else gx.at[chip, half, e], dst_ref=gx.at[chip, half, e],
-            send_sem=s_send.at[slot, e], recv_sem=s_recv.at[slot, e],
-            device_id=sib, device_id_type=MESH_ID,
-        )
-
-    def x_copy(shift, e):
-        chip = at(shift)
-        slot = (shift + zn) % zn
-        return pltpu.make_async_remote_copy(
-            src_ref=py.at[1 - core, chip, e], dst_ref=pd.at[chip, e],
-            send_sem=x_send.at[slot, e], recv_sem=x_recv.at[slot, e],
-            device_id=sib, device_id_type=MESH_ID,
-        )
-
-    for e in (0, 1):
-        for direction in (0, 1):
-            g_copy(direction, 0, e).start()
-    for e in (0, 1):
-        s_copy(0, e, True).start()
-
-    def compute(shifts):
-        chips = [at(shift) for shift in shifts]
-
-        def one(e, _):
-            rows = jnp.concatenate([gx[chip, half, e] for chip in chips for half in (0, 1)], axis=0)
-            hidden = jnp.dot(rows, wgu[e], preferred_element_type=jnp.float32)
-            gate = jnp.minimum(hidden[:, :256], 7.0)
-            up = jnp.clip(hidden[:, 256:], -7.0, 7.0)
-            act = ((up + 1.0) * gate * (1.0 / (1.0 + jnp.exp(-1.702 * gate)))).astype(jnp.bfloat16)
-            part = jnp.dot(act, wdn[e], preferred_element_type=jnp.float32).astype(jnp.bfloat16)
-            for number, chip in enumerate(chips):
-                for half in (0, 1):
-                    py[half, chip, e] = part[(2 * number + half) * 48:(2 * number + half) * 48 + 48]
-            return 0
-
-        lax.fori_loop(0, 2, one, 0)
-        for shift in shifts:
-            for e in (0, 1):
-                x_copy(shift, e).start()
-
-    for load in loads:
-        load.wait()
-    for e in (0, 1):
-        s_copy(0, e, False).wait_recv()
-    compute([0])
-
-    for hop in range(1, far + 1):
-        for e in (0, 1):
-            for direction in (0, 1):
-                if hop == far and e != direction:
-                    continue
-                g_wait(direction, hop, e)
-                if hop < far - 1 or (hop == far - 1 and e == direction):
-                    g_copy(direction, hop, e).start()
-                s_copy(-hop if direction == 0 else hop, e, True).start()
-        shifts = [-hop, hop] if hop < far else [far]
-        for shift in shifts:
-            for e in (0, 1):
-                s_copy(shift, e, False).wait_recv()
-        compute(shifts)
-
-    def pair_sum(shift, e):
-        chip = at(shift)
-        return py[core, chip, e].astype(jnp.float32) + pd[chip, e].astype(jnp.float32)
-
-    def r_copy(direction, hop, e):
-        return pltpu.make_async_remote_copy(
-            src_ref=rs_out.at[direction, hop, e], dst_ref=rs_in.at[direction, hop, e],
-            send_sem=r_send.at[direction, hop, e], recv_sem=r_recv.at[direction, hop, e],
-            device_id=z_up if direction == 0 else z_dn, device_id_type=MESH_ID,
-        )
-
-    seen = set()
-    used = []
-    for hop, flip in ((0, 0), (1, 1), (1, 0), (2, 1), (2, 0), (3, 1), (3, 0)):
-        for direction in (0, 1):
-            e = direction if flip == 0 else 1 - direction
-            shift = (far - hop) if direction == 0 else -(far - hop)
-            key = (shift % zn, e)
-            if key not in seen:
-                seen.add(key)
-                x_copy(shift, e).wait_recv()
-            total = pair_sum(shift, e)
-            if hop > 0 and not (hop == 1 and e != direction):
-                r_copy(direction, hop - 1, e).wait_recv()
-                total = total + rs_in[direction, hop - 1, e].astype(jnp.float32)
-            rs_out[direction, hop, e] = total.astype(jnp.bfloat16)
-            r_copy(direction, hop, e).start()
-            used.append((direction, hop, e))
-    for e in (0, 1):
-        x_copy(0, e).wait_recv()
-        total = pair_sum(0, e)
-        for direction in (0, 1):
-            r_copy(direction, far - 1, e).wait_recv()
-            total = total + rs_in[direction, far - 1, e].astype(jnp.float32)
-        out_ref[e] = total.astype(jnp.bfloat16)
-
-    for item in used:
-        r_copy(*item).wait_send()
-    for e in (0, 1):
-        for shift in range(-far + 1, far + 1):
-            s_copy(shift, e, True).wait_send()
-            x_copy(shift, e).wait_send()
-        for direction in (0, 1):
-            for hop in range(far):
-                if hop < far - 1 or e == direction:
-                    g_copy(direction, hop, e).wait_send()
-
-
-def run_experts(rows, gate_weight, up_weight, down_weight):
-    vmem = pl.BlockSpec(memory_space=pltpu.VMEM)
-    hbm = pl.BlockSpec(memory_space=pl.ANY)
-    bf16 = jnp.bfloat16
-    dma = pltpu.SemaphoreType.DMA
-    return pl.pallas_call(
-        expert_kernel,
-        out_shape=jax.ShapeDtypeStruct((2, 48, 2048), bf16),
-        in_specs=[vmem, hbm, hbm, hbm],
-        out_specs=vmem,
-        scratch_shapes=[
+        ]
+    scratch_b = [
+            pltpu.VMEM((16, 8, 2048), bf16), pltpu.VMEM((16, 8, 2048), bf16), pltpu.VMEM((16, 8, 2048), bf16),
+            pltpu.VMEM((2, 48, 2048), bf16),
             pltpu.VMEM((8, 2, 2, 48, 2048), bf16),
             pltpu.VMEM((2, 8, 2, 48, 2048), bf16),
             pltpu.VMEM((8, 2, 48, 2048), bf16),
@@ -593,12 +634,23 @@
             pltpu.VMEM((2, 256, 2048), bf16),
             pltpu.VMEM((2, 4, 2, 48, 2048), bf16),
             pltpu.VMEM((2, 4, 2, 48, 2048), bf16),
-            dma((4,)), dma((2, 4, 2)), dma((2, 4, 2)), dma((8, 2)), dma((8, 2)),
+            dma((16,)), dma((16,)), dma((16,)), dma((16,)),
+            dma((2, 4, 2)), dma((2, 4, 2)), dma((8, 2)), dma((8, 2)),
             dma((8, 2)), dma((8, 2)), dma((2, 4, 2)), dma((2, 4, 2)),
+        ]
+    assert len(scratch_a) == A_SCRATCH
+    return pl.pallas_call(
+        layer_kernel,
+        out_shape=jax.ShapeDtypeStruct((32, 2048), bf16),
+        in_specs=[hbm] * 20,
+        out_specs=vmem,
+        scratch_shapes=[
+            pltpu.VMEM((32, 2048), bf16), pltpu.VMEM((16, 8, 2048), bf16), pltpu.VMEM((32, 128), f32),
+            *scratch_a, dma((3,)), *scratch_b,
         ],
-        compiler_params=pltpu.CompilerParams(collective_id=2, has_side_effects=True, vmem_limit_bytes=56 * 2**20),
-        name="experts",
-    )(rows, gate_weight, up_weight, down_weight)
+        compiler_params=pltpu.CompilerParams(collective_id=1, has_side_effects=True, vmem_limit_bytes=67043328),
+        name="gather_attend_experts",
+    )(*args[:15], jnp.asarray(base), jnp.asarray(start), *args[15:])
 
 
 def body(
@@ -606,22 +658,11 @@
     key_up_second, value_up_second, out_first, out_second, residual, expert_gain,
     route_experts, route_scores, gate_weight, up_weight, down_weight,
 ):
-    middle, outgoing, mix = attend(
+    return layer(
         query_first.T, query_second.T, latent, key_rotary.T, latent_gain.reshape(1, -1), key_up_first.T, value_up_first.T,
         key_up_second, value_up_second, out_first, out_second, residual, expert_gain.reshape(1, -1),
-        route_experts.T, route_scores.T,
+        route_experts.T, route_scores.T, gate_weight, up_weight, down_weight,
     )
-    groups = lax.axis_size("sp")
-    local_experts = gate_weight.shape[0]
-    outgoing = outgoing.reshape(groups, local_experts, CAP, outgoing.shape[-1])
-    arrived = lax.all_to_all(outgoing, "sp", split_axis=0, concat_axis=0, tiled=True)
-    rows = arrived.transpose(1, 0, 2, 3).reshape(local_experts, groups * CAP, -1)
-    summed = run_experts(rows, gate_weight, up_weight, down_weight)
-    summed = summed.reshape(local_experts, groups, CAP, -1).transpose(1, 0, 2, 3)
-    returned = lax.all_to_all(summed, "sp", split_axis=0, concat_axis=0, tiled=True)
-    expert_out = returned.reshape(groups * local_experts * CAP, returned.shape[-1]).astype(jnp.float32)
-    mixture = jnp.dot(mix, expert_out)
-    return (middle.astype(jnp.float32) + mixture).astype(jnp.bfloat16)
 
 
 def solution(mesh):

time: 172 us -> 147 us (0.85)
  blocking collectives: 33.1 us -> 0 us
  Pallas kernels: 133 us -> 145 us
  local copies, waits for them, and re-layouts: 4.85 us -> 1.57 us
    all_to_all x2 -> x0, blocking collectives: 33.1 us -> none  [the longest x1 20.8 us: body(): lax.all_to_all(outgoing, 'sp', split_axis=0, concat_axis=0, tiled=True)]
    pallas_call x2 -> x1, Pallas kernels: 133 us -> 145 us  [layer(): pl.pallas_call(layer_kernel, out_shape=jax.ShapeDtypeStruct((32, 2048), b...]
    reshape x4 -> x0, local copies, waits for them, and re-layouts: 3.12 us -> none  [the longest x2 1.91 us: body(): outgoing = outgoing.reshape(groups, local_experts, CAP, outgoing.shape[-1])]
where the time goes in v3:
time: 147 us
  Pallas kernels  145 us (99%)
  local copies, waits for them, and re-layouts  1.57 us (1%)
    pallas_call x1, Pallas kernels, layer(): pl.pallas_call(layer_kernel, out_shape=jax.ShapeDtypeStruct((32, 2048), b...  145 us

profile of v3, /device:TPU:2, one launch (start us, length us, event | category | flops | bytes accessed | tf_op | source)
XLA Modules:
  0.0 146.9 jit_solution(9201274735026664787)
XLA Ops:
  0.0 145.4 %gather_attend_experts.1 = bf16[32,2048]{1,0:T(8,128)(2,1)} custom-call(bf16[96,512]{1,0:T(8,128)(2,1)} %bitcast.10, bf16[160,512]{1,0:T(8,128)(2,1)} %bitcast.9, bf16[512,512]{1,0:T(8,128)(2,1)} %refs_2_.1, bf16[32,512]{1,0:T(8,128)(2,1)} %bitcast.13, f32[1,512]{1,0:T(1,128)} %bitcast.17, bf16[64,512]{1,0:T(8,128)(2,1)} %bitcast.11, ...), custom_call_target="tpu_custom_call" | custom-call | tf_op jit(solution)/shard_map/gather_attend_experts/pallas_call | solution.py:642
  145.4 1.6 %copy.22 = bf16[32,2048]{1,0:T(8,128)(2,1)} copy(bf16[32,2048]{1,0:T(8,128)(2,1)} %gather_attend_experts.1) | data formatting | bytes 262144

commit v4 on v3

--- a/solution.py
+++ b/solution.py
@@ -295,7 +295,8 @@
         x_copy(d).start()
     project(core, po)
 
-    halves = (0, 1024)
+    width = 512
+    native = ((0, 1), (2, 3))
 
     def pair_sum(at, col, width):
         return po[at, :, pl.ds(col, width)].astype(jnp.float32) + pd[at, :, pl.ds(col, width)].astype(jnp.float32)
@@ -315,8 +316,8 @@
         if shift not in seen:
             x_copy(shift).wait_recv()
             seen.add(shift)
-        total = pair_sum(lax.rem(z + shift, zn), halves[part], 1024)
-        if hop > 0 and not (hop == 1 and part != direction):
+        total = pair_sum(lax.rem(z + shift, zn), part * width, width)
+        if hop > 0 and not (hop == 1 and part not in native[direction]):
             r_copy(direction, hop - 1, part).wait_recv()
             total = total + rs_in[direction, hop - 1, part].astype(jnp.float32)
         rs_out[direction, hop, part] = total.astype(jnp.bfloat16)
@@ -324,19 +325,20 @@
 
     used = []
     for hop, flip in ((0, 0), (1, 1), (1, 0), (2, 1), (2, 0), (3, 1), (3, 0)):
-        for direction in (0, 1):
-            part = direction if flip == 0 else 1 - direction
-            ring(direction, hop, part)
-            used.append((direction, hop, part))
+        for which in (0, 1):
+            for direction in (0, 1):
+                part = native[direction ^ flip][which]
+                ring(direction, hop, part)
+                used.append((direction, hop, part))
     x_copy(0).wait_recv()
     mids = []
-    for part in (0, 1):
-        total = pair_sum(z, halves[part], 1024)
+    for part in (0, 2, 1, 3):
+        total = pair_sum(z, part * width, width)
         for direction in (0, 1):
             r_copy(direction, far - 1, part).wait_recv()
             total = total + rs_in[direction, far - 1, part].astype(jnp.float32)
-        mids.append((res[:, pl.ds(halves[part], 1024)].astype(jnp.float32) + total).astype(jnp.bfloat16))
-    mid = jnp.concatenate(mids, axis=1)
+        mids.append((res[:, pl.ds(part * width, width)].astype(jnp.float32) + total).astype(jnp.bfloat16))
+    mid = jnp.concatenate([mids[0], mids[2], mids[1], mids[3]], axis=1)
     mid_ref[...] = mid
     wide = mid.astype(jnp.float32)
     normed = (wide * lax.rsqrt(jnp.mean(wide * wide, axis=1, keepdims=True) + EPS) * gain[...]).astype(bf16)
@@ -619,10 +621,10 @@
             pltpu.VMEM((8, 32, 2048), bf16),
             pltpu.VMEM((8, 32, 2048), bf16),
             pltpu.VMEM((8, 32, 2048), bf16),
-            pltpu.VMEM((2, 4, 2, 32, 1024), bf16),
-            pltpu.VMEM((2, 4, 2, 32, 1024), bf16),
+            pltpu.VMEM((2, 4, 4, 32, 512), bf16),
+            pltpu.VMEM((2, 4, 4, 32, 512), bf16),
             dma((20,)), dma((20,)), dma((15,)), dma((15,)), dma((17,)),
-            dma((8,)), dma((8,)), dma((2, 4, 2)), dma((2, 4, 2)),
+            dma((8,)), dma((8,)), dma((2, 4, 4)), dma((2, 4, 4)),
         ]
     scratch_b = [
             pltpu.VMEM((16, 8, 2048), bf16), pltpu.VMEM((16, 8, 2048), bf16), pltpu.VMEM((16, 8, 2048), bf16),

time: 147 us -> 147 us (level)
  no operation moved by 1% of the time
where the time goes in v4:
time: 147 us
  Pallas kernels  145 us (99%)
  local copies, waits for them, and re-layouts  1.57 us (1%)
    pallas_call x1, Pallas kernels, layer(): pl.pallas_call(layer_kernel, out_shape=jax.ShapeDtypeStruct((32, 2048), b...  145 us

profile of v4, /device:TPU:2, one launch (start us, length us, event | category | flops | bytes accessed | tf_op | source)
XLA Modules:
  0.0 146.5 jit_solution(7664748141782810940)
XLA Ops:
  0.0 144.9 %gather_attend_experts.1 = bf16[32,2048]{1,0:T(8,128)(2,1)} custom-call(bf16[96,512]{1,0:T(8,128)(2,1)} %bitcast.10, bf16[160,512]{1,0:T(8,128)(2,1)} %bitcast.9, bf16[512,512]{1,0:T(8,128)(2,1)} %refs_2_.1, bf16[32,512]{1,0:T(8,128)(2,1)} %bitcast.13, f32[1,512]{1,0:T(1,128)} %bitcast.17, bf16[64,512]{1,0:T(8,128)(2,1)} %bitcast.11, ...), custom_call_target="tpu_custom_call" | custom-call | tf_op jit(solution)/shard_map/gather_attend_experts/pallas_call | solution.py:644
  145.0 1.6 %copy.22 = bf16[32,2048]{1,0:T(8,128)(2,1)} copy(bf16[32,2048]{1,0:T(8,128)(2,1)} %gather_attend_experts.1) | data formatting | bytes 262144
